TPU v7x, 32 devices: a whole 2x2x4 slice. The times are simulated.
32 devices in a mesh: sp: 8 (over z, x), tp: 4 (over y, core).
Axes of the slice: x: 2, y: 2, z: 4, core: 2. Of those that a mesh axis runs over, the one named last changes fastest.
Arguments:
- tokens: bfloat16 [8192, 2048], P('sp', 'tp'), may hold values from -6 to 6
- norm_gain: float32 [2048], replicated, may hold values from 0.1 to 1.9
- att_query: bfloat16 [2048, 1024], P(None, 'tp'), may hold values from -1 to 1
- att_key: bfloat16 [2048, 512], P(None, 'tp'), may hold values from -16 to 16
- att_value: bfloat16 [2048, 512], P(None, 'tp'), may hold values from -0.125 to 0.125
- ret_query: bfloat16 [2048, 512], P(None, 'tp'), may hold values from -0.125 to 0.125
- ret_key: bfloat16 [2048, 512], P(None, 'tp'), may hold values from -0.125 to 0.125
- ret_value: bfloat16 [2048, 1024], P(None, 'tp'), may hold values from -0.125 to 0.125
- ret_gate: bfloat16 [2048, 1024], P(None, 'tp'), may hold values from -0.125 to 0.125
- att_sink: float32 [16], P('tp'), may hold values from 4 to 7
- decay_log: float32 [8, 8192], P('tp', 'sp'), may hold values from -2 to 0, as said below
- init_state: float32 [2, 8, 64, 128], P(None, 'tp'), may hold values from -24 to 24
- out_att: bfloat16 [1024, 2048], P('tp'), may hold values from -0.125 to 0.125
- out_ret: bfloat16 [1024, 2048], P('tp'), may hold values from -0.125 to 0.125
Outputs:
- mixed: bfloat16 [8192, 2048], P('sp', 'tp')
Inputs may be any that keep to these rules, and one draw needn't show every extreme that they name: `decay_log`: log decays, negative.
All inputs are finite; a program needn't handle non-finite values.
Results may differ from a plain program's by a relative error of at most 0.02.
Values may be sent and summed in bfloat16 or wider, within the bound.
A program may use at most 64 MiB of HBM per device.

v0:
```python
import jax
import jax.numpy as jnp
from jax import lax
from jax.sharding import PartitionSpec as P

HD = 64
RK = 64
RV = 128
WINDOW = 128
RET_BLOCK = 128


NORM_EPS = 1e-06
ROPE_BASE = 10000.0
HIGHEST = lax.Precision.HIGHEST


def padded_2(block, sides, width):
    for axis, dim in sides:
        count = lax.axis_size(axis)
        forward = [(i, i + 1) for i in range(count - 1)]
        backward = [(target, source) for source, target in forward]
        low = lax.ppermute(
            lax.slice_in_dim(block, block.shape[dim] - width, None, axis=dim), axis, forward
        )
        high = lax.ppermute(lax.slice_in_dim(block, 0, width, axis=dim), axis, backward)
        block = jnp.concatenate([low, block, high], axis=dim)
    return block


def passed_along(value, axis, by):
    length = lax.axis_size(axis)
    pairs = [(i, i + by) for i in range(length) if 0 <= i + by < length]
    return lax.ppermute(value, axis, pairs)


def rotated(values, positions):
    half_dim = values.shape[-1] // 2
    inverse = ROPE_BASE ** (-2.0 * jnp.arange(half_dim, dtype=jnp.float32) / values.shape[-1])
    angles = positions.astype(jnp.float32)[:, None] * inverse[None, :]
    cosine = jnp.cos(angles)[:, None, :]
    sine = jnp.sin(angles)[:, None, :]
    first_half = values[..., :half_dim]
    second_half = values[..., half_dim:]
    return jnp.concatenate(
        [first_half * cosine - second_half * sine, first_half * sine + second_half * cosine],
        axis=-1,
    )


def advance(state_now, item_pair):
    factor_now, term_now = item_pair
    return (factor_now[:, None, None] * state_now + term_now, state_now)


def body(
    tokens,
    norm_gain,
    att_query,
    att_key,
    att_value,
    ret_query,
    ret_key,
    ret_value,
    ret_gate,
    att_sink,
    decay_log,
    init_state,
    out_att,
    out_ret,
):
    tok_rows = tokens.shape[0]
    chan_local = tokens.shape[1]
    query_cols = att_query.shape[1]
    kv_cols = att_key.shape[1]
    rk_cols = ret_query.shape[1]
    rv_cols = ret_value.shape[1]
    heads_local = att_sink.shape[0]
    kv_local = kv_cols // HD
    groups = heads_local // kv_local
    ret_local = decay_log.shape[0]
    seq_offset = lax.axis_index("sp") * tok_rows
    seq_len = tok_rows * lax.axis_size("sp")
    joined = jnp.concatenate(
        [att_query, att_key, att_value, ret_query, ret_key, ret_value, ret_gate], axis=1
    )
    piece_f = lax.all_gather(tokens, "tp", axis=1, tiled=True).astype(jnp.float32)
    scaled = (piece_f * norm_gain[None, :]).astype(jnp.bfloat16)
    proj_sums = jnp.dot(scaled, joined, preferred_element_type=jnp.float32)
    squares = jnp.sum(piece_f * piece_f, axis=1)
    inv_rms = lax.rsqrt(squares / (chan_local * lax.axis_size("tp")) + NORM_EPS)
    projected = (proj_sums * inv_rms[:, None]).astype(jnp.bfloat16)
    off_rq = query_cols + 2 * kv_cols
    off_rk = off_rq + rk_cols
    off_rv = off_rk + rk_cols
    off_gate = off_rv + rv_cols
    key_vals = projected[:, query_cols:off_rq]
    padded = padded_2(key_vals, (("sp", 0),), WINDOW)
    block_rows = min(512, tok_rows)
    span_rows = block_rows + 2 * WINDOW
    queries = projected[:, :query_cols].reshape(tok_rows, kv_local, groups, HD)
    sink_col = att_sink.reshape(kv_local, groups, 1, 1)
    outputs = []
    for first_row in range(0, tok_rows, block_rows):
        query_block = queries[first_row : first_row + block_rows]
        span_block = padded[first_row : first_row + span_rows]
        key_block = span_block[:, :kv_cols].reshape(span_rows, kv_local, HD)
        value_block = span_block[:, kv_cols:].reshape(span_rows, kv_local, HD)
        scores = jnp.einsum(
            "qkgd,skd->kgqs", query_block, key_block, preferred_element_type=jnp.float32
        ) * HD ** (-0.5)
        query_pos = seq_offset + first_row + jnp.arange(block_rows, dtype=jnp.int32)
        key_pos = seq_offset + first_row - WINDOW + jnp.arange(span_rows, dtype=jnp.int32)
        allowed = (
            (jnp.abs(query_pos[:, None] - key_pos[None, :]) <= WINDOW)
            & (key_pos >= 0)[None, :]
            & (key_pos < seq_len)[None, :]
        )
        scores = jnp.where(allowed, scores, -jnp.inf)
        row_top = jnp.maximum(jnp.max(scores, axis=-1, keepdims=True), sink_col)
        raised = jnp.exp(scores - row_top)
        denominator = jnp.sum(raised, axis=-1, keepdims=True) + jnp.exp(sink_col - row_top)
        weights_bf = (raised / denominator).astype(jnp.bfloat16)
        block_out = jnp.einsum(
            "kgqs,skd->qkgd", weights_bf, value_block, preferred_element_type=jnp.float32
        )
        outputs.append(block_out.reshape(block_rows, query_cols).astype(jnp.bfloat16))
    attended = jnp.concatenate(outputs, axis=0)
    positions = seq_offset + jnp.arange(tok_rows, dtype=jnp.int32)
    query_rot = rotated(
        projected[:, off_rq:off_rk].astype(jnp.float32).reshape(tok_rows, ret_local, RK), positions
    )
    key_rot = rotated(
        projected[:, off_rk:off_rv].astype(jnp.float32).reshape(tok_rows, ret_local, RK), positions
    ) * RK ** (-0.5)
    value_f = projected[:, off_rv:off_gate].astype(jnp.float32).reshape(tok_rows, ret_local, RV)
    gate_f = projected[:, off_gate:].astype(jnp.float32)
    block_count = tok_rows // RET_BLOCK

    def heads_first(values, width):
        return jnp.transpose(values.reshape(block_count, RET_BLOCK, ret_local, width), (2, 0, 1, 3))

    query_h = heads_first(query_rot, RK)
    key_h = heads_first(key_rot, RK)
    value_h = heads_first(value_f, RV)
    block_logs = decay_log.reshape(ret_local, block_count, RET_BLOCK)
    cumul = jnp.cumsum(block_logs, axis=-1)
    block_log = cumul[..., -1]
    inner_w = jnp.einsum("hbnk,hbmk->hbnm", query_h, key_h, precision=HIGHEST) * jnp.exp(
        -jnp.abs(cumul[..., :, None] - cumul[..., None, :])
    )
    local_out = jnp.einsum("hbnm,hbmv->hbnv", inner_w, value_h, precision=HIGHEST)
    fwd_terms = jnp.einsum(
        "hbmk,hbmv->bhkv",
        key_h * jnp.exp(block_log[..., None] - cumul)[..., None],
        value_h,
        precision=HIGHEST,
    )
    bwd_terms = jnp.einsum(
        "hbmk,hbmv->bhkv", key_h * jnp.exp(cumul)[..., None], value_h, precision=HIGHEST
    )
    factors = jnp.exp(block_log).T
    zero_state = jnp.zeros((ret_local, RK, RV), jnp.float32)
    fwd_total, fwd_local = lax.scan(advance, zero_state, (factors, fwd_terms))
    bwd_total, bwd_local = lax.scan(advance, zero_state, (factors, bwd_terms), reverse=True)
    before_log = jnp.cumsum(block_log, axis=1) - block_log
    after_log = jnp.sum(block_log, axis=1, keepdims=True) - jnp.cumsum(block_log, axis=1)
    device_factor = jnp.exp(jnp.sum(block_log, axis=1))
    my_index = lax.axis_index("sp")
    axis_count = lax.axis_size("sp")

    def relay(turn_index, running):
        fwd_now, bwd_now = running
        sent_fwd = passed_along(
            (device_factor[:, None, None] * fwd_now + fwd_total).astype(jnp.bfloat16), "sp", 1
        ).astype(jnp.float32)
        sent_bwd = passed_along(
            (device_factor[:, None, None] * bwd_now + bwd_total).astype(jnp.bfloat16), "sp", -1
        ).astype(jnp.float32)
        return (
            jnp.where(my_index == 0, init_state[0], sent_fwd),
            jnp.where(my_index == axis_count - 1, init_state[1], sent_bwd),
        )

    fwd_start, bwd_start = lax.fori_loop(0, axis_count - 1, relay, (init_state[0], init_state[1]))
    fwd_in = fwd_local + jnp.exp(before_log).T[:, :, None, None] * fwd_start[None]
    bwd_in = bwd_local + jnp.exp(after_log).T[:, :, None, None] * bwd_start[None]
    cross_out = jnp.exp(cumul)[..., None] * jnp.einsum(
        "hbnk,bhkv->hbnv", query_h, fwd_in, precision=HIGHEST
    )
    cross_out = cross_out + jnp.exp(block_log[..., None] - cumul)[..., None] * jnp.einsum(
        "hbnk,bhkv->hbnv", query_h, bwd_in, precision=HIGHEST
    )
    combined = local_out + cross_out
    centered = combined - jnp.mean(combined, axis=-1, keepdims=True)
    normed = centered * lax.rsqrt(jnp.mean(centered * centered, axis=-1, keepdims=True) + NORM_EPS)
    retained = jnp.transpose(normed, (1, 2, 0, 3)).reshape(tok_rows, ret_local * RV)
    ret_out = (jax.nn.silu(gate_f) * retained).astype(jnp.bfloat16)
    contract_dims = (((0,), (1,)), ((), ()))
    att_part = lax.dot_general(out_att, attended, contract_dims, preferred_element_type=jnp.float32)
    summed = lax.psum_scatter(
        (
            att_part
            + lax.dot_general(out_ret, ret_out, contract_dims, preferred_element_type=jnp.float32)
        ).astype(jnp.bfloat16),
        "tp",
        scatter_dimension=0,
        tiled=True,
    ).astype(jnp.float32)
    return summed.T.astype(jnp.bfloat16)


def solution(mesh):
    in_specs = (
        P("sp", "tp"),
        P(),
        P(None, "tp"),
        P(None, "tp"),
        P(None, "tp"),
        P(None, "tp"),
        P(None, "tp"),
        P(None, "tp"),
        P(None, "tp"),
        P("tp"),
        P("tp", "sp"),
        P(None, "tp", None, None),
        P("tp", None),
        P("tp", None),
    )
    out_specs = P("sp", "tp")
    return jax.shard_map(body, mesh=mesh, in_specs=in_specs, out_specs=out_specs, check_vma=False)
```

profile of v0, /device:TPU:0, one launch (start us, length us, event | category | flops | bytes accessed | tf_op | source)
XLA Modules:
  0.0 275.6 jit_solution(15155859861386811351)
XLA Ops:
  7.3 1.3 max.32
  15.3 1.2 multiply_cosine_fusion
  16.5 1.4 fusion.16
  17.9 1.4 fusion.14
  19.3 2.4 constant_dynamic-update-slice_fusion.6
  21.8 2.0 constant_dynamic-update-slice_fusion.5
  23.7 1.9 constant_dynamic-update-slice_fusion.4
  27.6 1.1 constant_dynamic-update-slice_fusion.1
  29.9 16.3 %all-gather.2.cloned.1.call-done = bf16[1024,2048]{1,0:T(8,128)(2,1)} async-done(((bf16[1024,512]{1,0:T(8,128)(2,1)}), bf16[1024,2048]{1,0:T(8,128)(2,1)}) %all-gather.2.cloned.1.call-update) | async-done | bytes 4194320 | tf_op jit(solution)/shard_map/all_gather | solution.py:87
  46.1 3.1 %fusion.3 = f32[1024]{0:T(1024)S(1)} fusion(bf16[1024,2048]{1,0:T(8,128)(2,1)} %all-gather.2.cloned.1.call-done), kind=kLoop, calls=%fused_computation.15 | loop fusion | flops 6290432 | bytes 4198400 | tf_op jit(solution)/shard_map/reduce_sum | solution.py:90
  49.2 8.9 %multiply_convert_fusion = bf16[1024,1280]{1,0:T(8,128)(2,1)S(1)} fusion(bf16[2048,1280]{1,0:T(8,128)(2,1)} %constant_dynamic-update-slice_fusion, bf16[1024,2048]{1,0:T(8,128)(2,1)} %all-gather.2.cloned.1.call-done, f32[2048]{0:T(1024)S(1)} %copy-done.25, f32[1024]{0:T(1024)S(1)} %add_rsqrt_fusion), kind=kOutput, calls=%fused_computation.25 | convolution fusion | flops 5377622016 | bytes 12070912 | tf_op jit(solution)/shard_map/dot_general | solution.py:89
  60.6 1.1 copy.46
  61.7 4.0 %collective-permute-start.2 = (bf16[128,256]{1,0:T(8,128)(2,1)}, bf16[128,256]{1,0:T(8,128)(2,1)}, u32[]{:S(2)}, u32[]{:S(2)}) collective-permute-start(bf16[128,256]{1,0:T(8,128)(2,1)} %get-tuple-element.351), channel_id=1, source_target_pairs={{0,4},{4,8},{8,12},{12,16},{16,20},{20,24},{24,28},{1,5},{5,9},{9,... | collective-permute-start | bytes 196616 | tf_op jit(solution)/shard_map/ppermute | solution.py:23
  65.7 1.5 collective-permute-start.3
  67.5 1.1 multiply_subtract_fusion.1
  70.4 1.9 fusion.37
  72.4 13.0 %while.46 = (s32[]{:T(128)}, f32[2,64,128]{2,1,0:T(8,128)S(1)}, f32[8,2,64,128]{3,2,1,0:T(8,128)S(1)}, f32[8,2]{1,0:T(8,128)}, f32[8,2,64,128]{3,2,1,0:T(8,128)}, /*index=5*/s32[]{:T(128)}, s32[]{:T(128)}, s32[]{:T(128)}) while((s32[]{:T(128)}, f32[2,64,128]{2,1,0:T(8,128)S(1)}, f32[8,2,64,128]{3,2,1,0:T(8,128)S(1)}, ...), condition=%wide.region_11.12_spmd.clone, body=%wide.region_10.11_spmd.clone.sunk | while | flops 65540 | bytes 327832 | solution.py:165
  85.4 1.9 fusion.39
  87.4 13.0 %while.45 = (s32[]{:T(128)}, f32[2,64,128]{2,1,0:T(8,128)S(1)}, f32[8,2,64,128]{3,2,1,0:T(8,128)S(1)}, f32[8,2]{1,0:T(8,128)}, f32[8,2,64,128]{3,2,1,0:T(8,128)}, /*index=5*/s32[]{:T(128)}, s32[]{:T(128)}) while((s32[]{:T(128)}, f32[2,64,128]{2,1,0:T(8,128)S(1)}, f32[8,2,64,128]{3,2,1,0:T(8,128)S(1)}, f32[8,2]{1,0:T(8,128)}, ...), condition=%wide.region_7.8_spmd.clone, body=%wide.region_6.7_spmd.clone.sunk | while | flops 65539 | bytes 327812 | solution.py:164
  100.4 80.8 %while.44 = (s32[]{:T(128)}, f32[2,64,128]{2,1,0:T(8,128)S(1)}, f32[2,64,128]{2,1,0:T(8,128)S(1)}, pred[]{:T(512)}, f32[2,2,64,128]{3,2,1,0:T(8,128)S(1)}, /*ind...) while((s32[]{:T(128)}, f32[2,64,128]{2,1,0:T(8,128)S(1)}, ...), condition=%wide.region_13.14_spmd, body=%wide.region_12.13_spmd.sunk | while | flops 163842 | bytes 1179895 | solution.py:185
  100.4 1.4 add_convert_fusion.5
  101.9 1.3 collective-permute-start
  103.2 5.2 %collective-permute-start.1 = (bf16[2,64,128]{2,1,0:T(8,128)(2,1)}, bf16[2,64,128]{2,1,0:T(8,128)(2,1)S(1)}, u32[]{:S(2)}, u32[]{:S(2)}) collective-permute-start(bf16[2,64,128]{2,1,0:T(8,128)(2,1)} %get-tuple-element.505), channel_id=1, source_target_pairs={{0,4},{4,8},{8,12},{12,16},{16,20},{20,24},{24,28},{1,5},{5,9},{9,... | collective-permute-start | bytes 98312 | tf_op jit(solution)/shard_map/while/body/eval_jaxpr/ppermute | solution.py:34
  108.5 1.7 collective-permute-done.1
  111.6 1.4 add_convert_fusion.5
  113.0 1.3 collective-permute-start
  114.3 5.4 %collective-permute-start.1 = (bf16[2,64,128]{2,1,0:T(8,128)(2,1)}, bf16[2,64,128]{2,1,0:T(8,128)(2,1)S(1)}, u32[]{:S(2)}, u32[]{:S(2)}) collective-permute-start(bf16[2,64,128]{2,1,0:T(8,128)(2,1)} %get-tuple-element.505), channel_id=1, source_target_pairs={{0,4},{4,8},{8,12},{12,16},{16,20},{20,24},{24,28},{1,5},{5,9},{9,... | collective-permute-start | bytes 98312 | tf_op jit(solution)/shard_map/while/body/eval_jaxpr/ppermute | solution.py:34
  119.9 1.7 collective-permute-done.1
  123.1 1.4 add_convert_fusion.5
  124.5 1.3 collective-permute-start
  125.8 5.6 %collective-permute-start.1 = (bf16[2,64,128]{2,1,0:T(8,128)(2,1)}, bf16[2,64,128]{2,1,0:T(8,128)(2,1)S(1)}, u32[]{:S(2)}, u32[]{:S(2)}) collective-permute-start(bf16[2,64,128]{2,1,0:T(8,128)(2,1)} %get-tuple-element.505), channel_id=1, source_target_pairs={{0,4},{4,8},{8,12},{12,16},{16,20},{20,24},{24,28},{1,5},{5,9},{9,... | collective-permute-start | bytes 98312 | tf_op jit(solution)/shard_map/while/body/eval_jaxpr/ppermute | solution.py:34
  131.6 1.7 collective-permute-done.1
  134.7 1.4 add_convert_fusion.5
  136.1 1.3 collective-permute-start
  137.4 5.6 %collective-permute-start.1 = (bf16[2,64,128]{2,1,0:T(8,128)(2,1)}, bf16[2,64,128]{2,1,0:T(8,128)(2,1)S(1)}, u32[]{:S(2)}, u32[]{:S(2)}) collective-permute-start(bf16[2,64,128]{2,1,0:T(8,128)(2,1)} %get-tuple-element.505), channel_id=1, source_target_pairs={{0,4},{4,8},{8,12},{12,16},{16,20},{20,24},{24,28},{1,5},{5,9},{9,... | collective-permute-start | bytes 98312 | tf_op jit(solution)/shard_map/while/body/eval_jaxpr/ppermute | solution.py:34
  143.2 1.7 collective-permute-done.1
  146.3 1.4 add_convert_fusion.5
  147.7 1.3 collective-permute-start
  149.0 5.6 %collective-permute-start.1 = (bf16[2,64,128]{2,1,0:T(8,128)(2,1)}, bf16[2,64,128]{2,1,0:T(8,128)(2,1)S(1)}, u32[]{:S(2)}, u32[]{:S(2)}) collective-permute-start(bf16[2,64,128]{2,1,0:T(8,128)(2,1)} %get-tuple-element.505), channel_id=1, source_target_pairs={{0,4},{4,8},{8,12},{12,16},{16,20},{20,24},{24,28},{1,5},{5,9},{9,... | collective-permute-start | bytes 98312 | tf_op jit(solution)/shard_map/while/body/eval_jaxpr/ppermute | solution.py:34
  154.8 1.7 collective-permute-done.1
  158.0 1.4 add_convert_fusion.5
  159.4 1.3 collective-permute-start
  160.6 5.6 %collective-permute-start.1 = (bf16[2,64,128]{2,1,0:T(8,128)(2,1)}, bf16[2,64,128]{2,1,0:T(8,128)(2,1)S(1)}, u32[]{:S(2)}, u32[]{:S(2)}) collective-permute-start(bf16[2,64,128]{2,1,0:T(8,128)(2,1)} %get-tuple-element.505), channel_id=1, source_target_pairs={{0,4},{4,8},{8,12},{12,16},{16,20},{20,24},{24,28},{1,5},{5,9},{9,... | collective-permute-start | bytes 98312 | tf_op jit(solution)/shard_map/while/body/eval_jaxpr/ppermute | solution.py:34
  166.5 1.7 collective-permute-done.1
  169.6 1.4 add_convert_fusion.5
  171.0 1.3 collective-permute-start
  172.3 5.6 %collective-permute-start.1 = (bf16[2,64,128]{2,1,0:T(8,128)(2,1)}, bf16[2,64,128]{2,1,0:T(8,128)(2,1)S(1)}, u32[]{:S(2)}, u32[]{:S(2)}) collective-permute-start(bf16[2,64,128]{2,1,0:T(8,128)(2,1)} %get-tuple-element.505), channel_id=1, source_target_pairs={{0,4},{4,8},{8,12},{12,16},{16,20},{20,24},{24,28},{1,5},{5,9},{9,... | collective-permute-start | bytes 98312 | tf_op jit(solution)/shard_map/while/body/eval_jaxpr/ppermute | solution.py:34
  178.1 1.7 collective-permute-done.1
  182.1 1.8 fusion.29
  184.0 1.8 fusion.30
  185.8 2.0 convolution_multiply_fusion
  187.9 1.3 fusion.64
  189.8 1.8 fusion.66
  191.6 1.8 copy.41
  194.3 1.3 copy.57
  197.6 2.2 fusion.6
  200.0 1.4 fusion.4
  201.4 1.3 fusion.7
  202.8 1.4 fusion.5
  206.2 4.9 %fusion.17 = bf16[2,64,2,512]{3,1,2,0:T(8,128)(2,1)S(1)} fusion(bf16[768,2,64,1]{0,2,3,1:T(8,128)(2,1)} %bitcast.206, f32[2,768,512,2]{2,1,3,0:T(8,128)} %copy-done.2, f32[2,2,512]{2,1,0:T(2,128)S(1)} %exponential_add_fusion, f32[2,2,512]{2,1,0:T(2,128)S(1)} %get-tuple-element.381, pred[512,768]{0,1:T(8,128)(4,1)} %fusion.16), kind=kOutput, calls=%fused_computation.41 | convolution fusion | flops 209321984 | bytes 7159808 | tf_op jit(solution)/shard_map/kgqs,skd->qkgd/dot_general | solution.py:124
  211.1 1.9 fusion.18
  213.1 1.3 fusion.32
  214.6 4.4 %fusion.10 = bf16[2048,1024]{0,1:T(8,128)(2,1)} fusion(f32[1024,2048]{1,0:T(8,128)S(1)} %fusion.32, bf16[256,2048]{1,0:T(8,128)(2,1)S(1)} %copy-done.14, f32[128,8,2,128]{3,2,1,0:T(2,128)S(1)} %bitcast.193, bf16[1024,1280]{1,0:T(8,128)(2,1)} %copy-done.5), kind=kOutput, calls=%fused_computation.29 | convolution fusion | flops 1079771136 | bytes 15204352 | tf_op jit(solution)/shard_map/dot_general | solution.py:204
  219.1 49.7 %reduce-scatter.2.cloned.1.call-done = bf16[512,1024]{0,1:T(8,128)(2,1)} async-done(((bf16[2048,1024]{0,1:T(8,128)(2,1)}), bf16[512,1024]{0,1:T(8,128)(2,1)}) %reduce-scatter.2.cloned.1.call-update) | async-done | bytes 1048592 | tf_op jit(solution)/shard_map/reduce_scatter | solution.py:201
  (202 shorter events, 58.6 us)
Async XLA Ops:
  6.5 206.6 %copy-start = (bf16[256,2048]{1,0:T(8,128)(2,1)S(1)}, bf16[256,2048]{1,0:T(8,128)(2,1)}, u32[]{:S(2)}) copy-start(bf16[256,2048]{1,0:T(8,128)(2,1)} %param.32) | copy-start | bytes 3145732
  6.5 21.1 %copy-start.12 = (bf16[2048,256]{1,0:T(8,128)(2,1)S(1)}, bf16[2048,256]{1,0:T(8,128)(2,1)}, u32[]{:S(2)}) copy-start(bf16[2048,256]{1,0:T(8,128)(2,1)} %param.27) | copy-start | bytes 3145732
  6.5 22.2 %copy-start.13 = (bf16[2048,256]{1,0:T(8,128)(2,1)S(1)}, bf16[2048,256]{1,0:T(8,128)(2,1)}, u32[]{:S(2)}) copy-start(bf16[2048,256]{1,0:T(8,128)(2,1)} %param.28) | copy-start | bytes 3145732
  6.5 39.6 %all-gather.2.cloned.1.call-start = ((), (), s32[]{:S(2)}) async-start(), calls=%async_computation.1 | async-start | bytes 5242880 | tf_op jit(solution)/shard_map/all_gather | solution.py:87
  7.3 261.5 %reduce-scatter.2.cloned.1.call-start = ((), (), s32[]{:S(2)}) async-start(), calls=%async_computation.2 | async-start | bytes 5242880 | tf_op jit(solution)/shard_map/reduce_scatter | solution.py:201
  13.0 12.7 %copy-start.17 = (bf16[2048,128]{1,0:T(8,128)(2,1)S(1)}, bf16[2048,128]{1,0:T(8,128)(2,1)}, u32[]{:S(2)}) copy-start(bf16[2048,128]{1,0:T(8,128)(2,1)} %param.25) | copy-start | bytes 1572868
  13.0 13.7 %copy-start.18 = (bf16[2048,128]{1,0:T(8,128)(2,1)S(1)}, bf16[2048,128]{1,0:T(8,128)(2,1)}, u32[]{:S(2)}) copy-start(bf16[2048,128]{1,0:T(8,128)(2,1)} %param.26) | copy-start | bytes 1572868
  25.7 23.6 %copy-start.25 = (f32[2048]{0:T(1024)S(1)}, f32[2048]{0:T(1024)}, u32[]{:S(2)}) copy-start(f32[2048]{0:T(1024)} %param.21) | copy-start | bytes 24580
  58.2 1.8 copy-start.5
  61.7 133.9 %collective-permute-start.2 = (bf16[128,256]{1,0:T(8,128)(2,1)}, bf16[128,256]{1,0:T(8,128)(2,1)}, u32[]{:S(2)}, u32[]{:S(2)}) collective-permute-start(bf16[128,256]{1,0:T(8,128)(2,1)} %get-tuple-element.351), channel_id=1, source_target_pairs={{0,4},{4,8},{8,12},{12,16},{16,20},{20,24},{24,28},{1,5},{5,9},{9,... | collective-permute-start | bytes 196616 | tf_op jit(solution)/shard_map/ppermute | solution.py:23
  65.7 129.9 %collective-permute-start.3 = (bf16[128,256]{1,0:T(8,128)(2,1)}, bf16[128,256]{1,0:T(8,128)(2,1)}, u32[]{:S(2)}, u32[]{:S(2)}) collective-permute-start(bf16[128,256]{1,0:T(8,128)(2,1)} %get-tuple-element.352), channel_id=1, source_target_pairs={{4,0},{8,4},{12,8},{16,12},{20,16},{24,20},{28,24},{5,1},{9,5},{13... | collective-permute-start | bytes 196616 | tf_op jit(solution)/shard_map/ppermute | solution.py:26
  68.8 31.6 %copy-start.3 = (f32[2,2,64,128]{3,2,1,0:T(8,128)S(1)}, f32[2,2,64,128]{3,2,1,0:T(8,128)}, u32[]{:S(2)}) copy-start(f32[2,2,64,128]{3,2,1,0:T(8,128)} %param.31) | copy-start | bytes 393220
  100.4 85.4 %copy-start.6 = (f32[2,8,128,64]{2,1,3,0:T(8,128)S(1)}, f32[2,8,128,64]{2,1,3,0:T(8,128)}, u32[]{:S(2)}) copy-start(f32[2,8,128,64]{2,1,3,0:T(8,128)} %fusion.36) | copy-start | bytes 1572868
  101.9 6.6 %collective-permute-start = (bf16[2,64,128]{2,1,0:T(8,128)(2,1)}, bf16[2,64,128]{2,1,0:T(8,128)(2,1)S(1)}, u32[]{:S(2)}, u32[]{:S(2)}) collective-permute-start(bf16[2,64,128]{2,1,0:T(8,128)(2,1)} %get-tuple-element.504), channel_id=1, source_target_pairs={{4,0},{8,4},{12,8},{16,12},{20,16},{24,20},{28,24},{5,1},{9,5},{13... | collective-permute-start | bytes 98312 | tf_op jit(solution)/shard_map/while/body/eval_jaxpr/ppermute | solution.py:34
  103.2 7.1 %collective-permute-start.1 = (bf16[2,64,128]{2,1,0:T(8,128)(2,1)}, bf16[2,64,128]{2,1,0:T(8,128)(2,1)S(1)}, u32[]{:S(2)}, u32[]{:S(2)}) collective-permute-start(bf16[2,64,128]{2,1,0:T(8,128)(2,1)} %get-tuple-element.505), channel_id=1, source_target_pairs={{0,4},{4,8},{8,12},{12,16},{16,20},{20,24},{24,28},{1,5},{5,9},{9,... | collective-permute-start | bytes 98312 | tf_op jit(solution)/shard_map/while/body/eval_jaxpr/ppermute | solution.py:34
  108.5 1.7 copy-start.15
  110.2 0.6 copy-start.16
  113.0 6.9 %collective-permute-start = (bf16[2,64,128]{2,1,0:T(8,128)(2,1)}, bf16[2,64,128]{2,1,0:T(8,128)(2,1)S(1)}, u32[]{:S(2)}, u32[]{:S(2)}) collective-permute-start(bf16[2,64,128]{2,1,0:T(8,128)(2,1)} %get-tuple-element.504), channel_id=1, source_target_pairs={{4,0},{8,4},{12,8},{16,12},{20,16},{24,20},{28,24},{5,1},{9,5},{13... | collective-permute-start | bytes 98312 | tf_op jit(solution)/shard_map/while/body/eval_jaxpr/ppermute | solution.py:34
  114.3 7.3 %collective-permute-start.1 = (bf16[2,64,128]{2,1,0:T(8,128)(2,1)}, bf16[2,64,128]{2,1,0:T(8,128)(2,1)S(1)}, u32[]{:S(2)}, u32[]{:S(2)}) collective-permute-start(bf16[2,64,128]{2,1,0:T(8,128)(2,1)} %get-tuple-element.505), channel_id=1, source_target_pairs={{0,4},{4,8},{8,12},{12,16},{16,20},{20,24},{24,28},{1,5},{5,9},{9,... | collective-permute-start | bytes 98312 | tf_op jit(solution)/shard_map/while/body/eval_jaxpr/ppermute | solution.py:34
  119.9 1.7 copy-start.15
  121.7 0.6 copy-start.16
  124.5 7.1 %collective-permute-start = (bf16[2,64,128]{2,1,0:T(8,128)(2,1)}, bf16[2,64,128]{2,1,0:T(8,128)(2,1)S(1)}, u32[]{:S(2)}, u32[]{:S(2)}) collective-permute-start(bf16[2,64,128]{2,1,0:T(8,128)(2,1)} %get-tuple-element.504), channel_id=1, source_target_pairs={{4,0},{8,4},{12,8},{16,12},{20,16},{24,20},{28,24},{5,1},{9,5},{13... | collective-permute-start | bytes 98312 | tf_op jit(solution)/shard_map/while/body/eval_jaxpr/ppermute | solution.py:34
  125.8 7.5 %collective-permute-start.1 = (bf16[2,64,128]{2,1,0:T(8,128)(2,1)}, bf16[2,64,128]{2,1,0:T(8,128)(2,1)S(1)}, u32[]{:S(2)}, u32[]{:S(2)}) collective-permute-start(bf16[2,64,128]{2,1,0:T(8,128)(2,1)} %get-tuple-element.505), channel_id=1, source_target_pairs={{0,4},{4,8},{8,12},{12,16},{16,20},{20,24},{24,28},{1,5},{5,9},{9,... | collective-permute-start | bytes 98312 | tf_op jit(solution)/shard_map/while/body/eval_jaxpr/ppermute | solution.py:34
  131.6 1.7 copy-start.15
  133.3 0.6 copy-start.16
  136.1 7.1 %collective-permute-start = (bf16[2,64,128]{2,1,0:T(8,128)(2,1)}, bf16[2,64,128]{2,1,0:T(8,128)(2,1)S(1)}, u32[]{:S(2)}, u32[]{:S(2)}) collective-permute-start(bf16[2,64,128]{2,1,0:T(8,128)(2,1)} %get-tuple-element.504), channel_id=1, source_target_pairs={{4,0},{8,4},{12,8},{16,12},{20,16},{24,20},{28,24},{5,1},{9,5},{13... | collective-permute-start | bytes 98312 | tf_op jit(solution)/shard_map/while/body/eval_jaxpr/ppermute | solution.py:34
  137.4 7.5 %collective-permute-start.1 = (bf16[2,64,128]{2,1,0:T(8,128)(2,1)}, bf16[2,64,128]{2,1,0:T(8,128)(2,1)S(1)}, u32[]{:S(2)}, u32[]{:S(2)}) collective-permute-start(bf16[2,64,128]{2,1,0:T(8,128)(2,1)} %get-tuple-element.505), channel_id=1, source_target_pairs={{0,4},{4,8},{8,12},{12,16},{16,20},{20,24},{24,28},{1,5},{5,9},{9,... | collective-permute-start | bytes 98312 | tf_op jit(solution)/shard_map/while/body/eval_jaxpr/ppermute | solution.py:34
  143.2 1.7 copy-start.15
  144.9 0.6 copy-start.16
  147.7 7.1 %collective-permute-start = (bf16[2,64,128]{2,1,0:T(8,128)(2,1)}, bf16[2,64,128]{2,1,0:T(8,128)(2,1)S(1)}, u32[]{:S(2)}, u32[]{:S(2)}) collective-permute-start(bf16[2,64,128]{2,1,0:T(8,128)(2,1)} %get-tuple-element.504), channel_id=1, source_target_pairs={{4,0},{8,4},{12,8},{16,12},{20,16},{24,20},{28,24},{5,1},{9,5},{13... | collective-permute-start | bytes 98312 | tf_op jit(solution)/shard_map/while/body/eval_jaxpr/ppermute | solution.py:34
  149.0 7.5 %collective-permute-start.1 = (bf16[2,64,128]{2,1,0:T(8,128)(2,1)}, bf16[2,64,128]{2,1,0:T(8,128)(2,1)S(1)}, u32[]{:S(2)}, u32[]{:S(2)}) collective-permute-start(bf16[2,64,128]{2,1,0:T(8,128)(2,1)} %get-tuple-element.505), channel_id=1, source_target_pairs={{0,4},{4,8},{8,12},{12,16},{16,20},{20,24},{24,28},{1,5},{5,9},{9,... | collective-permute-start | bytes 98312 | tf_op jit(solution)/shard_map/while/body/eval_jaxpr/ppermute | solution.py:34
  154.8 1.7 copy-start.15
  156.6 0.6 copy-start.16
  159.4 7.1 %collective-permute-start = (bf16[2,64,128]{2,1,0:T(8,128)(2,1)}, bf16[2,64,128]{2,1,0:T(8,128)(2,1)S(1)}, u32[]{:S(2)}, u32[]{:S(2)}) collective-permute-start(bf16[2,64,128]{2,1,0:T(8,128)(2,1)} %get-tuple-element.504), channel_id=1, source_target_pairs={{4,0},{8,4},{12,8},{16,12},{20,16},{24,20},{28,24},{5,1},{9,5},{13... | collective-permute-start | bytes 98312 | tf_op jit(solution)/shard_map/while/body/eval_jaxpr/ppermute | solution.py:34
  160.6 7.5 %collective-permute-start.1 = (bf16[2,64,128]{2,1,0:T(8,128)(2,1)}, bf16[2,64,128]{2,1,0:T(8,128)(2,1)S(1)}, u32[]{:S(2)}, u32[]{:S(2)}) collective-permute-start(bf16[2,64,128]{2,1,0:T(8,128)(2,1)} %get-tuple-element.505), channel_id=1, source_target_pairs={{0,4},{4,8},{8,12},{12,16},{16,20},{20,24},{24,28},{1,5},{5,9},{9,... | collective-permute-start | bytes 98312 | tf_op jit(solution)/shard_map/while/body/eval_jaxpr/ppermute | solution.py:34
  166.5 1.7 copy-start.15
  168.2 0.6 copy-start.16
  171.0 7.1 %collective-permute-start = (bf16[2,64,128]{2,1,0:T(8,128)(2,1)}, bf16[2,64,128]{2,1,0:T(8,128)(2,1)S(1)}, u32[]{:S(2)}, u32[]{:S(2)}) collective-permute-start(bf16[2,64,128]{2,1,0:T(8,128)(2,1)} %get-tuple-element.504), channel_id=1, source_target_pairs={{4,0},{8,4},{12,8},{16,12},{20,16},{24,20},{28,24},{5,1},{9,5},{13... | collective-permute-start | bytes 98312 | tf_op jit(solution)/shard_map/while/body/eval_jaxpr/ppermute | solution.py:34
  172.3 7.5 %collective-permute-start.1 = (bf16[2,64,128]{2,1,0:T(8,128)(2,1)}, bf16[2,64,128]{2,1,0:T(8,128)(2,1)S(1)}, u32[]{:S(2)}, u32[]{:S(2)}) collective-permute-start(bf16[2,64,128]{2,1,0:T(8,128)(2,1)} %get-tuple-element.505), channel_id=1, source_target_pairs={{0,4},{4,8},{8,12},{12,16},{16,20},{20,24},{24,28},{1,5},{5,9},{9,... | collective-permute-start | bytes 98312 | tf_op jit(solution)/shard_map/while/body/eval_jaxpr/ppermute | solution.py:34
  178.1 1.7 copy-start.15
  179.8 0.6 copy-start.16
  181.2 6.6 %copy-start.8 = (bf16[8,128,2,128]{1,3,0,2:T(8,128)(2,1)S(1)}, bf16[8,128,2,128]{1,3,0,2:T(8,128)(2,1)}, u32[]{:S(2)}) copy-start(bf16[8,128,2,128]{1,3,0,2:T(8,128)(2,1)} %copy.46) | copy-start | bytes 1572868
  181.2 6.6 %copy-start.21 = (f32[2,8,128]{2,1,0:T(8,128)S(1)}, f32[2,8,128]{2,1,0:T(8,128)}, u32[]{:S(2)}) copy-start(f32[2,8,128]{2,1,0:T(8,128)} %get-tuple-element.374) | copy-start | bytes 24580
  184.0 5.4 %copy-start.22 = (f32[8,128,2]{1,0,2:T(8,128)S(1)}, f32[8,128,2]{1,0,2:T(8,128)}, u32[]{:S(2)}) copy-start(f32[8,128,2]{1,0,2:T(8,128)} %get-tuple-element.369) | copy-start | bytes 24580
  184.0 5.4 %copy-start.23 = (f32[8,128,2]{1,0,2:T(8,128)S(1)}, f32[8,128,2]{1,0,2:T(8,128)}, u32[]{:S(2)}) copy-start(f32[8,128,2]{1,0,2:T(8,128)} %get-tuple-element.370) | copy-start | bytes 24580
  189.2 6.4 %copy-start.7 = (bf16[1024,256]{1,0:T(8,128)(2,1)S(1)}, bf16[1024,256]{1,0:T(8,128)(2,1)}, u32[]{:S(2)}) copy-start(bf16[1024,256]{1,0:T(8,128)(2,1)} %get-tuple-element.348) | copy-start | bytes 1572868
  189.4 8.2 %copy-start.9 = (pred[512,768]{0,1:T(8,128)(4,1)S(1)}, pred[512,768]{0,1:T(8,128)(4,1)}, u32[]{:S(2)}) copy-start(pred[512,768]{0,1:T(8,128)(4,1)} %fusion.14) | copy-start | bytes 1179652
  195.6 4.3 %copy-start.24 = (f32[2,2]{1,0:T(2,128)S(1)}, f32[2,2]{1,0:T(2,128)}, u32[]{:S(2)}) copy-start(f32[2,2]{1,0:T(2,128)} %max.32) | copy-start | bytes 52
  199.8 2.8 %copy-start.1 = (f32[2,768,512,2]{2,1,3,0:T(8,128)}, f32[2,768,512,2]{2,1,3,0:T(8,128)S(1)}, u32[]{:S(2)}) copy-start(f32[2,768,512,2]{2,1,3,0:T(8,128)S(1)} %get-tuple-element.383) | copy-start | bytes 18874372
  199.9 1.5 copy-start.11
  199.9 1.5 copy-start.19
  202.7 2.6 copy-start.2
  205.3 5.8 %slice-start = ((s8[6291456]{0:T(1024)(128)(4,1)}), s8[2097152]{0:T(1024)(128)(4,1)S(1)}, s32[]{:S(2)}) async-start(s8[6291456]{0:T(1024)(128)(4,1)} %bitcast.191), calls=%async_computation.3 | async-start | bytes 4194304
  206.2 4.9 %slice-start.1 = ((s8[6291456]{0:T(1024)(128)(4,1)}), s8[4194304]{0:T(1024)(128)(4,1)S(1)}, s32[]{:S(2)}) async-start(s8[6291456]{0:T(1024)(128)(4,1)} %bitcast.191), calls=%async_computation.4 | async-start | bytes 8388608
  206.2 5.0 %copy-start.10 = (pred[512,768]{0,1:T(8,128)(4,1)S(1)}, pred[512,768]{0,1:T(8,128)(4,1)}, u32[]{:S(2)}) copy-start(pred[512,768]{0,1:T(8,128)(4,1)} %fusion.14) | copy-start | bytes 1179652
  206.2 5.0 %copy-start.20 = (bf16[768,128]{0,1:T(8,128)(2,1)S(1)}, bf16[768,128]{0,1:T(8,128)(2,1)}, u32[]{:S(2)}) copy-start(bf16[768,128]{0,1:T(8,128)(2,1)} %copy.35) | copy-start | bytes 589828
  213.1 1.3 copy-start.4
  213.1 1.5 copy-start.14
Sparse Core Ops, SparseCore 0:
  8.9 37.1 all-gather.1
  219.2 49.4 reduce-scatter.1
where the time goes:
time: 278 us; the launch traced here: 276 us
  waiting for transfers between devices  79.9 us (29%)
  starting transfers between devices  53.3 us (19%)
  other arithmetic  47.7 us (17%)
  local copies, waits for them, and re-layouts  44.5 us (16%)
  matrix products  35.8 us (13%)
  between operations  14 us (5%)
    reduce_scatter x1, waiting for transfers between devices, body(): lax.psum_scatter((att_part + lax.dot_general(out_ret, ret_out, contract_d...  49.7 us
    ppermute x14, starting transfers between devices, passed_along(): return lax.ppermute(value, axis, pairs)  47.8 us
    all_gather x1, waiting for transfers between devices, body(): lax.all_gather(tokens, 'tp', axis=1, tiled=True).astype(jnp.float32)  16.3 us
    add x16, other arithmetic, advance(): return (factor_now[:, None, None] * state_now + term_now, state_now)  14.6 us
    ppermute x14, waiting for transfers between devices, passed_along(): return lax.ppermute(value, axis, pairs)  13.2 us
    unnamed x62, local copies, waits for them, and re-layouts  12.4 us
    mul x16, local copies, waits for them, and re-layouts, advance(): return (factor_now[:, None, None] * state_now + term_now, state_now)  11.1 us
    convert_element_type x7, other arithmetic, relay(): (device_factor[:, None, None] * bwd_now + bwd_total).astype(jnp.bfloat16)  9.74 us
  transfers between devices with their start and end apart: 18, of which 16 were waited for; matrix products, arithmetic and copies ran while one was open for 31% of the time, Pallas kernels for 0%

commit v1 on v0

--- a/solution.py
+++ b/solution.py
@@ -28,12 +28,6 @@
     return block
 
 
-def passed_along(value, axis, by):
-    length = lax.axis_size(axis)
-    pairs = [(i, i + by) for i in range(length) if 0 <= i + by < length]
-    return lax.ppermute(value, axis, pairs)
-
-
 def rotated(values, positions):
     half_dim = values.shape[-1] // 2
     inverse = ROPE_BASE ** (-2.0 * jnp.arange(half_dim, dtype=jnp.float32) / values.shape[-1])
@@ -46,11 +40,6 @@
         [first_half * cosine - second_half * sine, first_half * sine + second_half * cosine],
         axis=-1,
     )
-
-
-def advance(state_now, item_pair):
-    factor_now, term_now = item_pair
-    return (factor_now[:, None, None] * state_now + term_now, state_now)
 
 
 def body(
@@ -159,30 +148,34 @@
     bwd_terms = jnp.einsum(
         "hbmk,hbmv->bhkv", key_h * jnp.exp(cumul)[..., None], value_h, precision=HIGHEST
     )
-    factors = jnp.exp(block_log).T
-    zero_state = jnp.zeros((ret_local, RK, RV), jnp.float32)
-    fwd_total, fwd_local = lax.scan(advance, zero_state, (factors, fwd_terms))
-    bwd_total, bwd_local = lax.scan(advance, zero_state, (factors, bwd_terms), reverse=True)
-    before_log = jnp.cumsum(block_log, axis=1) - block_log
-    after_log = jnp.sum(block_log, axis=1, keepdims=True) - jnp.cumsum(block_log, axis=1)
-    device_factor = jnp.exp(jnp.sum(block_log, axis=1))
     my_index = lax.axis_index("sp")
     axis_count = lax.axis_size("sp")
-
-    def relay(turn_index, running):
-        fwd_now, bwd_now = running
-        sent_fwd = passed_along(
-            (device_factor[:, None, None] * fwd_now + fwd_total).astype(jnp.bfloat16), "sp", 1
-        ).astype(jnp.float32)
-        sent_bwd = passed_along(
-            (device_factor[:, None, None] * bwd_now + bwd_total).astype(jnp.bfloat16), "sp", -1
-        ).astype(jnp.float32)
-        return (
-            jnp.where(my_index == 0, init_state[0], sent_fwd),
-            jnp.where(my_index == axis_count - 1, init_state[1], sent_bwd),
-        )
-
-    fwd_start, bwd_start = lax.fori_loop(0, axis_count - 1, relay, (init_state[0], init_state[1]))
+    upto = jnp.cumsum(block_log, axis=1)
+    before_log = upto - block_log
+    total_log = upto[:, -1:]
+    after_log = total_log - upto
+    order = jnp.arange(block_count)
+    earlier = order[None, :] < order[:, None]
+    fwd_w = jnp.where(earlier, jnp.exp(jnp.where(earlier, before_log[:, :, None] - upto[:, None, :], 0.0)), 0.0)
+    later = order[None, :] > order[:, None]
+    bwd_w = jnp.where(later, jnp.exp(jnp.where(later, before_log[:, None, :] - upto[:, :, None], 0.0)), 0.0)
+    fwd_local = jnp.einsum("hba,ahkv->bhkv", fwd_w, fwd_terms, precision=HIGHEST)
+    bwd_local = jnp.einsum("hba,ahkv->bhkv", bwd_w, bwd_terms, precision=HIGHEST)
+    fwd_total = jnp.einsum("ha,ahkv->hkv", jnp.exp(after_log), fwd_terms, precision=HIGHEST)
+    bwd_total = jnp.einsum("ha,ahkv->hkv", jnp.exp(before_log), bwd_terms, precision=HIGHEST)
+    totals = lax.all_gather(jnp.stack([fwd_total, bwd_total]).astype(jnp.bfloat16), "sp").astype(jnp.float32)
+    logs = lax.all_gather(total_log[:, 0], "sp")
+    dev = jnp.arange(axis_count)
+    dev_upto = jnp.cumsum(logs, axis=0)
+    dev_before = dev_upto - logs
+    mine_before = lax.dynamic_index_in_dim(dev_before, my_index, 0)
+    mine_upto = lax.dynamic_index_in_dim(dev_upto, my_index, 0)
+    is_low = (dev < my_index)[:, None]
+    is_high = (dev > my_index)[:, None]
+    low_w = jnp.where(is_low, jnp.exp(jnp.where(is_low, mine_before - dev_upto, 0.0)), 0.0)
+    high_w = jnp.where(is_high, jnp.exp(jnp.where(is_high, dev_before - mine_upto, 0.0)), 0.0)
+    fwd_start = jnp.einsum("dh,dhkv->hkv", low_w, totals[:, 0], precision=HIGHEST) + jnp.exp(mine_before[0])[:, None, None] * init_state[0]
+    bwd_start = jnp.einsum("dh,dhkv->hkv", high_w, totals[:, 1], precision=HIGHEST) + jnp.exp(dev_upto[-1] - mine_upto[0])[:, None, None] * init_state[1]
     fwd_in = fwd_local + jnp.exp(before_log).T[:, :, None, None] * fwd_start[None]
     bwd_in = bwd_local + jnp.exp(after_log).T[:, :, None, None] * bwd_start[None]
     cross_out = jnp.exp(cumul)[..., None] * jnp.einsum(

time: 278 us -> 205 us (0.74)
  blocking collectives: 0 us -> 54.6 us
  starting transfers between devices: 53.3 us -> 3.22 us
  waiting for transfers between devices: 79.9 us -> 45.1 us
  other arithmetic: 47.7 us -> 20.3 us
  local copies, waits for them, and re-layouts: 44.5 us -> 28 us
    ppermute x14 -> x0, starting transfers between devices: 47.8 us -> none  [passed_along(): return lax.ppermute(value, axis, pairs)]
    all_gather x0 -> x1, blocking collectives: none -> 31.5 us  [body(): lax.all_gather(jnp.stack([fwd_total, bwd_total]).astype(jnp.bfloat16), 'sp')]
    unnamed x0 -> x1, blocking collectives: none -> 23.1 us
    all_gather x1, waiting for transfers between devices: 16.3 us -> 0.01 us  [body(): lax.all_gather(tokens, 'tp', axis=1, tiled=True).astype(jnp.float32)]
    add x17 -> x1, other arithmetic: 15.5 us -> 0.08 us  [body(): jnp.einsum('dh,dhkv->hkv', low_w, totals[:, 0], precision=HIGHEST)]
    ppermute x14 -> x0, waiting for transfers between devices: 13.2 us -> none  [passed_along(): return lax.ppermute(value, axis, pairs)]
    mul x16 -> x0, local copies, waits for them, and re-layouts: 11.1 us -> none  [advance(): return (factor_now[:, None, None] * state_now + term_now, state_now)]
    convert_element_type x7 -> x0, other arithmetic: 9.74 us -> none  [relay(): (device_factor[:, None, None] * bwd_now + bwd_total).astype(jnp.bfloat16)]
  transfers between devices with their start and end apart: 18 -> 4, of which waited for: 16 -> 1; matrix products, arithmetic and copies ran while one was open for 31% -> 22% of each run, Pallas kernels for 0% -> 0%
where the time goes in v1:
time: 205 us; the launch traced here: 204 us
  blocking collectives  54.6 us (27%)
  waiting for transfers between devices  45.1 us (22%)
  matrix products  38.4 us (19%)
  local copies, waits for them, and re-layouts  28 us (14%)
  other arithmetic  20.3 us (10%)
  between operations  14.8 us (7%)
  starting transfers between devices  3.22 us (2%)
    reduce_scatter x1, waiting for transfers between devices, body(): lax.psum_scatter((att_part + lax.dot_general(out_ret, ret_out, contract_d...  44.3 us
    all_gather x1, blocking collectives, body(): lax.all_gather(jnp.stack([fwd_total, bwd_total]).astype(jnp.bfloat16), 'sp')  31.5 us
    unnamed x1, blocking collectives  23.1 us
    unnamed x84, local copies, waits for them, and re-layouts  11.8 us
    dot_general x1, matrix products, body(): proj_sums = jnp.dot(scaled, joined, preferred_element_type=jnp.float32)  8.95 us
    dot_general x2, matrix products, body(): jnp.einsum('kgqs,skd->qkgd', weights_bf, value_block, preferred_element_t...  6.88 us
    dot_general x1, matrix products, body(): lax.dot_general(out_ret, ret_out, contract_dims, preferred_element_type=j...  4.4 us
  transfers between devices with their start and end apart: 4, of which 1 were waited for; matrix products, arithmetic and copies ran while one was open for 22% of the time, Pallas kernels for 0%

profile of v1, /device:TPU:0, one launch (start us, length us, event | category | flops | bytes accessed | tf_op | source)
XLA Modules:
  0.0 204.4 jit_solution(8675876458490304616)
XLA Ops:
  6.5 0.7 all-gather.3.cloned.1.call-update
  7.3 0.7 copy.140
  8.0 0.6 reduce_window_sum.37
  8.9 1.2 dynamic-slice
  11.2 23.1 %all-reduce = f32[16]{0:T(128)S(1)} all-reduce(f32[16]{0:T(128)S(1)} %dynamic-update-slice), channel_id=2, replica_groups=mesh['sp'=8,'tp'=4] {'sp'}, use_global_device_ids=true, to_apply=%add | all-reduce | flops 16 | bytes 128
  34.4 1.3 max.32
  35.8 0.6 fusion.90
  36.4 0.5 fusion.103
  37.0 0.6 copy.85
  37.6 0.6 exponential_bitcast_fusion
  38.8 0.7 copy.89
  39.5 0.5 iota_compare_fusion
  40.1 0.6 iota_compare_fusion.1
  40.7 0.7 subtract_reduce_fusion
  41.4 0.6 subtract_exponential_fusion.2
  42.0 0.7 bitcast_exponential_fusion
  42.7 1.2 multiply_cosine_fusion
  43.9 1.4 fusion.14
  45.3 0.7 fusion.12
  46.1 2.4 %constant_dynamic-update-slice_fusion.6 = bf16[2048,1280]{1,0:T(8,128)(2,1)} fusion(bf16[2048,256]{1,0:T(8,128)(2,1)} %param.16), kind=kLoop, calls=%fused_computation.115 | loop fusion | bytes 2097152
  48.5 1.9 constant_dynamic-update-slice_fusion.5
  50.4 1.9 constant_dynamic-update-slice_fusion.4
  52.3 0.9 constant_dynamic-update-slice_fusion.3
  53.2 0.9 constant_dynamic-update-slice_fusion.2
  54.1 1.2 constant_dynamic-update-slice_fusion.1
  55.3 1.2 constant_dynamic-update-slice_fusion
  56.5 3.1 %fusion.1 = f32[1024]{0:T(1024)S(1)} fusion(bf16[1024,2048]{1,0:T(8,128)(2,1)} %all-gather.3.cloned.1.call-done), kind=kLoop, calls=%fused_computation.3 | loop fusion | flops 6290432 | bytes 4198400 | tf_op jit(solution)/shard_map/reduce_sum | solution.py:79
  59.6 9.0 %multiply_convert_fusion = bf16[1024,1280]{1,0:T(8,128)(2,1)S(1)} fusion(bf16[2048,1280]{1,0:T(8,128)(2,1)} %constant_dynamic-update-slice_fusion, bf16[1024,2048]{1,0:T(8,128)(2,1)} %all-gather.3.cloned.1.call-done, f32[2048]{0:T(1024)} %param.15, f32[1024]{0:T(1024)S(1)} %add_rsqrt_fusion), kind=kOutput, calls=%fused_computation.13 | convolution fusion | flops 5377622016 | bytes 12070912 | tf_op jit(solution)/shard_map/dot_general | solution.py:78
  68.5 1.0 fusion.104
  69.6 0.7 fusion.106
  70.9 1.1 copy.61
  72.0 1.9 collective-permute-start
  73.9 1.3 collective-permute-start.1
  75.6 1.1 multiply_subtract_fusion
  76.9 0.9 fusion.58
  77.8 1.1 fusion.37
  78.9 0.8 fusion.48
  79.8 1.1 fusion.39
  80.9 0.8 fusion.51
  81.7 31.5 %all_gather.12 = bf16[8,2,2,64,128]{4,3,2,1,0:T(8,128)(2,1)S(1)} all-gather(bf16[1,2,2,64,128]{4,3,2,1,0:T(8,128)(2,1)S(1)} %pad_maximum_fusion.4), channel_id=1, replica_groups=mesh['sp'=8,'tp'=4] {'sp'}, dimensions={0}, use_global_device_ids=true | all-gather | bytes 589824 | tf_op jit(solution)/shard_map/all_gather | solution.py:166
  114.1 2.0 convolution_multiply_fusion
  116.3 0.9 fusion.16
  117.2 1.8 fusion.29
  119.1 0.9 fusion.15
  120.0 1.8 fusion.30
  121.8 1.3 fusion.102
  123.8 1.1 fusion.105
  124.9 0.8 copy.54
  125.7 0.8 copy.50
  126.5 1.3 copy.71
  127.9 1.6 pad_maximum_fusion.2
  129.4 0.8 copy.52
  130.6 2.2 %fusion.4 = (f32[2,2,512]{2,1,0:T(2,128)S(1)}, f32[2,768,512,2]{2,1,3,0:T(8,128)S(1)}) fusion(pred[512,768]{0,1:T(8,128)(4,1)S(1)} %fusion.12, bf16[768,2,64,1]{0,2,3,1:T(8,128)(2,1)S(1)} %bitcast.235, bf16[512,2,2,64]{0,3,2,1:T(8,128)(2,1)} %bitcast.229), kind=kOutput, calls=%fused_computation.14 | convolution fusion | flops 206043136 | bytes 7151616 | tf_op jit(solution)/shard_map/qkgd,skd->kgqs/dot_general | solution.py:98
  132.9 1.4 fusion.2
  134.3 1.3 fusion.5
  135.6 0.8 exponential_add_fusion.1
  136.4 1.4 fusion.3
  137.8 0.7 exponential_add_fusion
  138.5 1.9 copy.48
  140.4 5.0 %fusion.17 = bf16[2,64,2,512]{3,1,2,0:T(8,128)(2,1)S(1)} fusion(bf16[768,2,64,1]{0,2,3,1:T(8,128)(2,1)} %bitcast.232, f32[2,768,512,2]{2,1,3,0:T(8,128)} %copy-done.2, f32[2,2,512]{2,1,0:T(2,128)} %exponential_add_fusion, f32[2,2,512]{2,1,0:T(2,128)S(1)} %get-tuple-element.51, pred[512,768]{0,1:T(8,128)(4,1)} %fusion.14), kind=kOutput, calls=%fused_computation.33 | convolution fusion | flops 209321984 | bytes 7159808 | tf_op jit(solution)/shard_map/kgqs,skd->qkgd/dot_general | solution.py:113
  145.4 1.9 fusion.18
  147.3 1.3 fusion.32
  148.8 4.4 %fusion.8 = bf16[2048,1024]{0,1:T(8,128)(2,1)} fusion(f32[1024,2048]{1,0:T(8,128)S(1)} %fusion.32, bf16[256,2048]{1,0:T(8,128)(2,1)S(1)} %copy-done.10, f32[128,8,2,128]{3,2,1,0:T(2,128)S(1)} %bitcast.221, bf16[1024,1280]{1,0:T(8,128)(2,1)} %copy-done.4), kind=kOutput, calls=%fused_computation.17 | convolution fusion | flops 1079771136 | bytes 15204352 | tf_op jit(solution)/shard_map/dot_general | solution.py:197
  153.3 44.3 %reduce-scatter.2.cloned.1.call-done = bf16[512,1024]{0,1:T(8,128)(2,1)} async-done(((bf16[2048,1024]{0,1:T(8,128)(2,1)}), bf16[512,1024]{0,1:T(8,128)(2,1)}) %reduce-scatter.2.cloned.1.call-update) | async-done | bytes 1048592 | tf_op jit(solution)/shard_map/reduce_scatter | solution.py:194
  (122 shorter events, 5.2 us)
Async XLA Ops:
  6.5 140.8 %copy-start = (bf16[256,2048]{1,0:T(8,128)(2,1)S(1)}, bf16[256,2048]{1,0:T(8,128)(2,1)}, u32[]{:S(2)}) copy-start(bf16[256,2048]{1,0:T(8,128)(2,1)} %param.26) | copy-start | bytes 3145732
  6.5 47.5 %copy-start.8 = (bf16[2048,256]{1,0:T(8,128)(2,1)S(1)}, bf16[2048,256]{1,0:T(8,128)(2,1)}, u32[]{:S(2)}) copy-start(bf16[2048,256]{1,0:T(8,128)(2,1)} %param.21) | copy-start | bytes 3145732
  6.5 48.7 %copy-start.9 = (bf16[2048,256]{1,0:T(8,128)(2,1)S(1)}, bf16[2048,256]{1,0:T(8,128)(2,1)}, u32[]{:S(2)}) copy-start(bf16[2048,256]{1,0:T(8,128)(2,1)} %param.22) | copy-start | bytes 3145732
  6.5 49.9 %all-gather.3.cloned.1.call-start = ((), (), s32[]{:S(2)}) async-start(), calls=%async_computation.1 | async-start | bytes 5242880 | tf_op jit(solution)/shard_map/all_gather | solution.py:76
  7.3 190.3 %reduce-scatter.2.cloned.1.call-start = ((), (), s32[]{:S(2)}) async-start(), calls=%async_computation.2 | async-start | bytes 5242880 | tf_op jit(solution)/shard_map/reduce_scatter | solution.py:194
  8.9 36.4 %copy-start.19 = (f32[2,8]{1,0:T(2,128)}, f32[2,8]{1,0:T(2,128)S(1)}, u32[]{:S(2)}) copy-start(f32[2,8]{1,0:T(2,128)S(1)} %reduce_window_sum.39) | copy-start | bytes 196
  38.3 1.2 copy-start.23
  39.5 12.8 %copy-start.11 = (bf16[2048,128]{1,0:T(8,128)(2,1)S(1)}, bf16[2048,128]{1,0:T(8,128)(2,1)}, u32[]{:S(2)}) copy-start(bf16[2048,128]{1,0:T(8,128)(2,1)} %param.19) | copy-start | bytes 1572868
  39.5 13.7 %copy-start.12 = (bf16[2048,128]{1,0:T(8,128)(2,1)S(1)}, bf16[2048,128]{1,0:T(8,128)(2,1)}, u32[]{:S(2)}) copy-start(bf16[2048,128]{1,0:T(8,128)(2,1)} %param.20) | copy-start | bytes 1572868
  68.5 1.8 copy-start.4
  72.0 55.8 %collective-permute-start = (bf16[128,256]{1,0:T(8,128)(2,1)}, bf16[128,256]{1,0:T(8,128)(2,1)}, u32[]{:S(2)}, u32[]{:S(2)}) collective-permute-start(bf16[128,256]{1,0:T(8,128)(2,1)} %get-tuple-element.21), channel_id=1, source_target_pairs={{0,4},{4,8},{8,12},{12,16},{16,20},{20,24},{24,28},{1,5},{5,9},{9,... | collective-permute-start | bytes 196616 | tf_op jit(solution)/shard_map/ppermute | solution.py:23
  73.9 53.9 %collective-permute-start.1 = (bf16[128,256]{1,0:T(8,128)(2,1)}, bf16[128,256]{1,0:T(8,128)(2,1)}, u32[]{:S(2)}, u32[]{:S(2)}) collective-permute-start(bf16[128,256]{1,0:T(8,128)(2,1)} %get-tuple-element.22), channel_id=1, source_target_pairs={{4,0},{8,4},{12,8},{16,12},{20,16},{24,20},{28,24},{5,1},{9,5},{13... | collective-permute-start | bytes 196616 | tf_op jit(solution)/shard_map/ppermute | solution.py:26
  75.6 3.3 %copy-start.28 = (f32[2,8]{1,0:T(2,128)S(1)}, f32[2,8]{1,0:T(2,128)}, u32[]{:S(2)}) copy-start(f32[2,8]{1,0:T(2,128)} %exp.98) | copy-start | bytes 196
  75.6 5.3 %copy-start.22 = (f32[2,8]{1,0:T(2,128)S(1)}, f32[2,8]{1,0:T(2,128)}, u32[]{:S(2)}) copy-start(f32[2,8]{1,0:T(2,128)} %get-tuple-element.49) | copy-start | bytes 196
  75.6 37.7 %copy-start.26 = (f32[8,2,1,1]{0,2,3,1:T(1,128)S(1)}, f32[8,2,1,1]{0,2,3,1:T(1,128)}, u32[]{:S(2)}) copy-start(f32[8,2,1,1]{0,2,3,1:T(1,128)} %copy.85) | copy-start | bytes 196
  75.6 38.1 %copy-start.27 = (f32[8,2,1,1]{0,2,3,1:T(1,128)S(1)}, f32[8,2,1,1]{0,2,3,1:T(1,128)}, u32[]{:S(2)}) copy-start(f32[8,2,1,1]{0,2,3,1:T(1,128)} %copy.89) | copy-start | bytes 196
  76.9 39.3 %copy-start.15 = (f32[2,2,64,128]{3,2,1,0:T(8,128)S(1)}, f32[2,2,64,128]{3,2,1,0:T(8,128)}, u32[]{:S(2)}) copy-start(f32[2,2,64,128]{3,2,1,0:T(8,128)} %param.25) | copy-start | bytes 393220
  76.9 39.3 %copy-start.31 = (f32[2]{0:T(128)S(1)}, f32[2]{0:T(128)}, u32[]{:S(2)}) copy-start(f32[2]{0:T(128)} %get-tuple-element.11) | copy-start | bytes 28
  76.9 39.3 %copy-start.32 = (f32[2]{0:T(128)S(1)}, f32[2]{0:T(128)}, u32[]{:S(2)}) copy-start(f32[2]{0:T(128)} %get-tuple-element.9) | copy-start | bytes 28
  77.7 38.5 %copy-start.20 = (f32[2,8]{1,0:T(2,128)S(1)}, f32[2,8]{1,0:T(2,128)}, u32[]{:S(2)}) copy-start(f32[2,8]{1,0:T(2,128)} %copy-done.19) | copy-start | bytes 196
  77.8 38.5 %copy-start.24 = (f32[2,8]{1,0:T(2,128)S(1)}, f32[2,8]{1,0:T(2,128)}, u32[]{:S(2)}) copy-start(f32[2,8]{1,0:T(2,128)} %copy-done.23) | copy-start | bytes 196
  77.8 38.5 %copy-start.34 = (pred[8,8]{1,0:T(8,128)(4,1)S(1)}, pred[8,8]{1,0:T(8,128)(4,1)}, u32[]{:S(2)}) copy-start(pred[8,8]{1,0:T(8,128)(4,1)} %iota_compare_fusion) | copy-start | bytes 196
  79.7 39.3 %copy-start.29 = (f32[2,8]{1,0:T(2,128)S(1)}, f32[2,8]{1,0:T(2,128)}, u32[]{:S(2)}) copy-start(f32[2,8]{1,0:T(2,128)} %subtract_reduce_fusion) | copy-start | bytes 196
  79.7 39.3 %copy-start.30 = (f32[8,2]{0,1:T(2,128)S(1)}, f32[8,2]{0,1:T(2,128)}, u32[]{:S(2)}) copy-start(f32[8,2]{0,1:T(2,128)} %get-tuple-element.7) | copy-start | bytes 196
  79.8 39.3 %copy-start.33 = (pred[8,8]{1,0:T(8,128)(4,1)S(1)}, pred[8,8]{1,0:T(8,128)(4,1)}, u32[]{:S(2)}) copy-start(pred[8,8]{1,0:T(8,128)(4,1)} %iota_compare_fusion.1) | copy-start | bytes 196
  113.2 8.6 %copy-start.6 = (bf16[8,128,2,128]{1,3,0,2:T(8,128)(2,1)S(1)}, bf16[8,128,2,128]{1,3,0,2:T(8,128)(2,1)}, u32[]{:S(2)}) copy-start(bf16[8,128,2,128]{1,3,0,2:T(8,128)(2,1)} %copy.61) | copy-start | bytes 1572868
  113.2 8.6 %copy-start.16 = (f32[2,8,128]{2,1,0:T(8,128)S(1)}, f32[2,8,128]{2,1,0:T(8,128)}, u32[]{:S(2)}) copy-start(f32[2,8,128]{2,1,0:T(8,128)} %get-tuple-element.46) | copy-start | bytes 24580
  119.0 4.3 %copy-start.17 = (f32[8,128,2]{1,0,2:T(8,128)S(1)}, f32[8,128,2]{1,0,2:T(8,128)}, u32[]{:S(2)}) copy-start(f32[8,128,2]{1,0,2:T(8,128)} %get-tuple-element.41) | copy-start | bytes 24580
  119.0 4.3 %copy-start.18 = (f32[8,128,2]{1,0,2:T(8,128)S(1)}, f32[8,128,2]{1,0,2:T(8,128)}, u32[]{:S(2)}) copy-start(f32[8,128,2]{1,0,2:T(8,128)} %get-tuple-element.42) | copy-start | bytes 24580
  123.1 4.7 %copy-start.5 = (bf16[1024,256]{1,0:T(8,128)(2,1)S(1)}, bf16[1024,256]{1,0:T(8,128)(2,1)}, u32[]{:S(2)}) copy-start(bf16[1024,256]{1,0:T(8,128)(2,1)} %get-tuple-element.18) | copy-start | bytes 1572868
  127.8 5.0 %copy-start.21 = (f32[2,2]{1,0:T(2,128)S(1)}, f32[2,2]{1,0:T(2,128)}, u32[]{:S(2)}) copy-start(f32[2,2]{1,0:T(2,128)} %max.32) | copy-start | bytes 52
  132.8 2.8 %copy-start.1 = (f32[2,768,512,2]{2,1,3,0:T(8,128)}, f32[2,768,512,2]{2,1,3,0:T(8,128)S(1)}, u32[]{:S(2)}) copy-start(f32[2,768,512,2]{2,1,3,0:T(8,128)S(1)} %get-tuple-element.53) | copy-start | bytes 18874372
  132.8 1.5 copy-start.7
  132.8 1.5 copy-start.13
  135.6 2.8 %copy-start.2 = (f32[2,768,512,2]{2,1,3,0:T(8,128)}, f32[2,768,512,2]{2,1,3,0:T(8,128)S(1)}, u32[]{:S(2)}) copy-start(f32[2,768,512,2]{2,1,3,0:T(8,128)S(1)} %get-tuple-element.55) | copy-start | bytes 18874372
  138.5 6.8 %slice-start = ((s8[6291456]{0:T(1024)(128)(4,1)}), s8[2097152]{0:T(1024)(128)(4,1)S(1)}, s32[]{:S(2)}) async-start(s8[6291456]{0:T(1024)(128)(4,1)} %bitcast.219), calls=%async_computation.3 | async-start | bytes 4194304
  140.3 5.0 %slice-start.1 = ((s8[6291456]{0:T(1024)(128)(4,1)}), s8[4194304]{0:T(1024)(128)(4,1)S(1)}, s32[]{:S(2)}) async-start(s8[6291456]{0:T(1024)(128)(4,1)} %bitcast.219), calls=%async_computation.4 | async-start | bytes 8388608
  140.3 5.0 %copy-start.14 = (bf16[768,128]{0,1:T(8,128)(2,1)S(1)}, bf16[768,128]{0,1:T(8,128)(2,1)}, u32[]{:S(2)}) copy-start(bf16[768,128]{0,1:T(8,128)(2,1)} %copy.48) | copy-start | bytes 589828
  140.4 5.0 %copy-start.25 = (f32[2,2,512]{2,1,0:T(2,128)S(1)}, f32[2,2,512]{2,1,0:T(2,128)}, u32[]{:S(2)}) copy-start(f32[2,2,512]{2,1,0:T(2,128)} %get-tuple-element.50) | copy-start | bytes 24580
  147.3 1.3 copy-start.3
  147.3 1.5 copy-start.10
Sparse Core Ops, SparseCore 0:
  8.9 37.2 all-gather.2
  153.4 44.1 reduce-scatter.1

commit v2 on v1

v2 whole, which is shorter than its diff:
```python
import functools

import jax
import jax.numpy as jnp
import numpy as np
from jax import lax
from jax.experimental import pallas as pl
from jax.experimental.pallas import tpu as pltpu
from jax.sharding import PartitionSpec as P

HD = 64
RK = 64
RV = 128
WINDOW = 128
CHUNK = 256
NORM_EPS = 1e-06
ROPE_BASE = 10000.0
F32 = jnp.float32
BF16 = jnp.bfloat16
MESH = pl.DeviceIdType.MESH


def rope_tables(count, step, heads):
    half = RK // 2
    inverse = ROPE_BASE ** (-2.0 * np.arange(half, dtype=np.float64) / RK)
    angles = (np.arange(count, dtype=np.float64) * step)[:, None] * inverse[None, :]
    wide = np.tile(np.concatenate([angles, angles], axis=1), (1, heads))
    return np.cos(wide).astype(np.float32), np.sin(wide).astype(np.float32)


def remote(src, dst, send, recv, **where):
    return pltpu.make_async_remote_copy(
        src_ref=src, dst_ref=dst, send_sem=send, recv_sem=recv,
        device_id=where, device_id_type=MESH,
    )


def rows_of(index, size):
    return pl.ds(pl.multiple_of(index * size, size), size)


def mm(a, b):
    return jnp.dot(a, b, preferred_element_type=F32)


def mm_t(a, b):
    return lax.dot_general(a, b, (((1,), (1,)), ((), ())), preferred_element_type=F32)


def tm_m(a, b):
    return lax.dot_general(a, b, (((0,), (0,)), ((), ())), preferred_element_type=F32)


def kernel(cfg, *refs):
    (tokens, gain, w_q, w_k, w_v, w_rq, w_rk, w_rv, w_rg, sink, decay, init, o_att, o_ret,
     outer_cos, outer_sin, inner_cos, inner_sin, out) = refs[:19]
    n_buf = len(cfg["buffers"])
    w_bufs = refs[19:19 + n_buf]
    (w_out, gath, xbuf, qs, kbuf, vbuf, att, qfb, rloc, gs, fterm, bterm, blog, tot_f, tot_b,
     tots, logs, states, acc, s_part, r_part, s_cross, r_cross,
     w_sem, wo_sem, tok_sem, ag_send, ag_recv, halo_send, halo_recv, tot_send, tot_recv,
     log_send, log_recv, part_send, part_recv, cross_send, cross_recv) = refs[19 + n_buf:]
    n_tp, n_sp, n_chips, chunks = cfg["n_tp"], cfg["n_sp"], cfg["n_chips"], cfg["chunks"]
    chan, heads, ret, kv = cfg["chan"], cfg["heads"], cfg["ret"], cfg["kv"]
    rows = chunks * CHUNK
    width = n_tp * chan
    groups = heads // kv
    seq_len = rows * n_sp
    sp = lax.axis_index("sp")
    tp = lax.axis_index("tp")
    core = lax.rem(tp, 2)
    chip = lax.div(tp, 2)
    partner = chip * 2 + 1 - core

    def across(k):
        return lax.rem(chip + k, n_chips) * 2 + core

    token_copy = pltpu.make_async_copy(tokens, gath.at[tp], tok_sem)
    token_copy.start()
    weights = (w_q, w_k, w_v, w_rq, w_rk, w_rv, w_rg)
    w_copies = []
    for i, (w_ref, (b, off, cols)) in enumerate(zip(weights, cfg["places"])):
        dst = w_bufs[b].at[:, pl.ds(off, cols)] if cfg["joined"] else w_bufs[b]
        w_copies.append(pltpu.make_async_copy(w_ref, dst, w_sem.at[i]))
    for copy in w_copies:
        copy.start()
    o_copies = []
    half_rows = heads * HD
    for j in range(n_tp):
        for part, (src, first, count) in enumerate(
            ((o_att, 0, half_rows), (o_ret, half_rows, ret * RV))
        ):
            o_copies.append(pltpu.make_async_copy(
                src.at[:, pl.ds(j * chan, chan)], w_out.at[j, pl.ds(first, count), :],
                wo_sem.at[j, part]))
    for copy in o_copies:
        copy.start()

    barrier = pltpu.get_barrier_semaphore()
    for k in range(1, n_tp):
        pl.semaphore_signal(barrier, inc=1, device_id={"tp": lax.rem(tp + k, n_tp)}, device_id_type=MESH)
    for k in range(1, n_sp):
        pl.semaphore_signal(barrier, inc=1, device_id={"sp": lax.rem(sp + k, n_sp)}, device_id_type=MESH)
    pl.semaphore_wait(barrier, n_tp - 1 + n_sp - 1)

    def own_cross(c, k):
        return remote(tokens.at[rows_of(c, CHUNK), :], gath.at[tp, rows_of(c, CHUNK), :],
                      ag_send.at[k, c], ag_recv.at[tp, c], tp=across(k))

    def own_part(c):
        return remote(tokens.at[rows_of(c, CHUNK), :], gath.at[tp, rows_of(c, CHUNK), :],
                      ag_send.at[0, c], ag_recv.at[tp, c], tp=partner)

    def arrival(c, slot, k=0):
        return remote(gath.at[slot, rows_of(c, CHUNK), :], gath.at[slot, rows_of(c, CHUNK), :],
                      ag_send.at[k, c], ag_recv.at[slot, c], tp=partner)

    def start_sends(c, carry):
        for k in range(1, n_chips):
            own_cross(c, k).start()
        own_part(c).start()
        return carry

    lax.fori_loop(0, chunks, start_sends, 0)

    for h in range(ret):
        total = jnp.sum(decay[h:h + 1, :], axis=1, keepdims=True)
        logs[sp, h] = jnp.broadcast_to(total, (8, 128))

    def log_copy(k):
        return remote(logs.at[sp], logs.at[sp], log_send.at[k], log_recv.at[sp],
                      sp=lax.rem(sp + k, n_sp))

    def log_arrival(k):
        other = lax.rem(sp + k, n_sp)
        return remote(logs.at[other], logs.at[other], log_send.at[k], log_recv.at[other], sp=other)

    token_copy.wait()
    for copy in w_copies:
        copy.wait()

    row_i = lax.broadcasted_iota(jnp.int32, (CHUNK, CHUNK), 0)
    col_i = lax.broadcasted_iota(jnp.int32, (CHUNK, CHUNK), 1)
    rw = ret * RK
    p_row = lax.broadcasted_iota(jnp.int32, (rw, rw), 0)
    p_col = lax.broadcasted_iota(jnp.int32, (rw, rw), 1)
    first_half = lax.rem(p_col, RK) < RK // 2
    swap = jnp.where(
        first_half & (p_row == p_col + RK // 2), -1.0,
        jnp.where(jnp.logical_not(first_half) & (p_row == p_col - RK // 2), 1.0, 0.0),
    ).astype(BF16)

    def attend(i):
        here = rows_of(i, 128)
        span = pl.ds(pl.multiple_of(i * 128, 128), 128 + 2 * WINDOW)
        shape = (128, 128 + 2 * WINDOW)
        q_i = lax.broadcasted_iota(jnp.int32, shape, 0)
        k_i = lax.broadcasted_iota(jnp.int32, shape, 1)
        key_pos = k_i + (sp * rows + i * 128 - WINDOW)
        allowed = (k_i >= q_i) & (k_i <= q_i + 2 * WINDOW) & (key_pos >= 0) & (key_pos < seq_len)
        allowed = jnp.concatenate([allowed.astype(F32)] * groups, axis=0) > 0.5
        done = []
        for g in range(kv):
            query = jnp.concatenate(
                [qs[here, (g * groups + j) * HD:(g * groups + j + 1) * HD] for j in range(groups)], axis=0)
            key = kbuf[span, g * HD:(g + 1) * HD]
            value = vbuf[span, g * HD:(g + 1) * HD]
            scores = jnp.where(allowed, mm_t(query, key), -jnp.inf)
            sink_col = jnp.concatenate(
                [jnp.full((128, 1), sink[g * groups + j], F32) for j in range(groups)], axis=0)
            top = jnp.maximum(jnp.max(scores, axis=1, keepdims=True), sink_col)
            raised = jnp.exp(scores - top)
            denominator = jnp.sum(raised, axis=1, keepdims=True) + jnp.exp(sink_col - top)
            result = mm(raised.astype(BF16), value) / denominator
            for j in range(groups):
                done.append(result[j * 128:(j + 1) * 128])
        att[here, :] = jnp.concatenate(done, axis=1).astype(BF16)

    def chunk_body(c, carry):
        here = rows_of(c, CHUNK)
        for k in range(1, n_chips):
            slot = across(k)
            arrival(c, slot).wait_recv()
            arrival(c, slot, n_chips - 1 + k).start()
        arrival(c, partner).wait_recv()
        for k in range(1, n_chips):
            arrival(c, lax.rem(chip + k, n_chips) * 2 + 1 - core).wait_recv()
        squares = jnp.zeros((CHUNK, 1), F32)
        for s in range(n_tp):
            piece = gath[s, here, :].astype(F32)
            squares = squares + jnp.sum(piece * piece, axis=1, keepdims=True)
            xbuf[:, s * chan:(s + 1) * chan] = (piece * gain[0:1, s * chan:(s + 1) * chan]).astype(BF16)
        inv_rms = lax.rsqrt(squares / width + NORM_EPS)
        found = {}
        for b, first, cols, names in cfg["dots"]:
            block = (mm(xbuf[...], w_bufs[b][:, first:first + cols]) * inv_rms).astype(BF16)
            at = 0
            for name, count in names:
                found[name] = block[:, at:at + count]
                at += count
        qs[here, :] = found["q"] * jnp.asarray(HD ** -0.5, BF16)
        shifted = pl.ds(pl.multiple_of(c * CHUNK + WINDOW, 128), CHUNK)
        kbuf[shifted, :] = found["k"]
        vbuf[shifted, :] = found["v"]
        gs[here, :] = found["g"]
        place = sp * chunks + c
        oc, os_ = outer_cos[pl.ds(place, 1), :], outer_sin[pl.ds(place, 1), :]
        ic, is_ = inner_cos[...], inner_sin[...]
        cosine = oc * ic - os_ * is_
        sine = os_ * ic + oc * is_
        query_rot = found["rq"].astype(F32) * cosine + mm(found["rq"], swap) * sine
        key_rot = (found["rk"].astype(F32) * cosine + mm(found["rk"], swap) * sine) * RK ** -0.5
        for h in range(ret):
            log_row = decay[h:h + 1, here]
            wide = jnp.broadcast_to(log_row, (CHUNK, CHUNK))
            log_col = jnp.sum(jnp.where(row_i == col_i, wide, 0.0), axis=1, keepdims=True)
            cum_col = jnp.sum(jnp.where(col_i <= row_i, wide, 0.0), axis=1, keepdims=True)
            cum_row = jnp.sum(jnp.where(row_i <= col_i, log_col, 0.0), axis=0, keepdims=True)
            total = jnp.sum(log_row, axis=1, keepdims=True)
            query = query_rot[:, h * RK:(h + 1) * RK]
            key = key_rot[:, h * RK:(h + 1) * RK]
            value = found["rv"][:, h * RV:(h + 1) * RV]
            inner = mm_t(query.astype(BF16), key.astype(BF16)) * jnp.exp(-jnp.abs(cum_col - cum_row))
            rloc[h, here, :] = mm(inner.astype(BF16), value)
            up = jnp.exp(cum_col)
            down = jnp.exp(jnp.minimum(total - cum_col, 0.0))
            qfb[h, here, :] = jnp.concatenate([query * up, query * down], axis=1).astype(BF16)
            both = jnp.concatenate([key * down, key * up], axis=1).astype(BF16)
            terms = tm_m(both, value)
            fterm[h, c] = terms[:RK]
            bterm[h, c] = terms[RK:]
            blog[h, c] = jnp.broadcast_to(total, (8, 128))

        @pl.when(c > 0)
        def _():
            attend(2 * c - 1)
            attend(2 * c)

        @pl.when(c == 0)
        def _():
            for k in range(1, n_sp):
                log_copy(k).start()

        return carry

    lax.fori_loop(0, chunks, chunk_body, 0)

    for h in range(ret):
        state = jnp.zeros((RK, RV), F32)
        back = jnp.zeros((RK, RV), F32)
        for c in range(chunks):
            state = jnp.exp(blog[h, c, 0:1, :]) * state + fterm[h, c]
            back = jnp.exp(blog[h, chunks - 1 - c, 0:1, :]) * back + bterm[h, chunks - 1 - c]
        tot_f[h] = state.astype(BF16)
        tot_b[h] = back.astype(BF16)

    left = lax.rem(sp + n_sp - 1, n_sp)
    right = lax.rem(sp + 1, n_sp)
    halos = []
    for i, buf in enumerate((kbuf, vbuf)):
        halos.append(remote(buf.at[pl.ds(rows, WINDOW), :], buf.at[pl.ds(0, WINDOW), :],
                            halo_send.at[0, i], halo_recv.at[0, i], sp=right))
        halos.append(remote(buf.at[pl.ds(WINDOW, WINDOW), :], buf.at[pl.ds(rows + WINDOW, WINDOW), :],
                            halo_send.at[1, i], halo_recv.at[1, i], sp=left))
    for copy in halos:
        copy.start()

    def send_f(d, carry):
        remote(tot_f, tots.at[sp], tot_send.at[d], tot_recv.at[sp], sp=d).start()
        return carry

    def send_b(d, carry):
        remote(tot_b, tots.at[sp], tot_send.at[d], tot_recv.at[sp], sp=d).start()
        return carry

    lax.fori_loop(sp + 1, n_sp, send_f, 0)
    lax.fori_loop(0, sp, send_b, 0)

    for copy in halos:
        copy.wait()
    attend(0)
    attend(2 * chunks - 1)
    for copy in o_copies:
        copy.wait()

    for k in range(1, n_sp):
        log_arrival(k).wait_recv()

    def total_arrival(e):
        return remote(tots.at[e], tots.at[e], tot_send.at[e], tot_recv.at[e], sp=e)

    for h in range(ret):
        states[0, h] = init[0, h]
        states[1, h] = init[1, h]

    def from_low(e, carry):
        total_arrival(e).wait_recv()
        for h in range(ret):
            states[0, h] = jnp.exp(logs[e, h, 0:1, :]) * states[0, h] + tots[e, h].astype(F32)
        return carry

    def from_high(i, carry):
        e = n_sp - 1 - i
        total_arrival(e).wait_recv()
        for h in range(ret):
            states[1, h] = jnp.exp(logs[e, h, 0:1, :]) * states[1, h] + tots[e, h].astype(F32)
        return carry

    lax.fori_loop(0, sp, from_low, 0)
    lax.fori_loop(0, n_sp - 1 - sp, from_high, 0)

    for h in range(ret):
        state = states[0, h]
        back = states[1, h]
        for c in range(chunks):
            term = fterm[h, c]
            fterm[h, c] = state
            state = jnp.exp(blog[h, c, 0:1, :]) * state + term
            r = chunks - 1 - c
            term = bterm[h, r]
            bterm[h, r] = back
            back = jnp.exp(blog[h, r, 0:1, :]) * back + term

    def part_copy(k, c):
        return remote(s_part.at[k, rows_of(c, CHUNK), :], r_part.at[k, rows_of(c, CHUNK), :],
                      part_send.at[k, c], part_recv.at[k, c], tp=partner)

    def cross_copy(k, c):
        return remote(s_cross.at[k - 1, rows_of(c, CHUNK), :],
                      r_cross.at[n_chips - k - 1, rows_of(c, CHUNK), :],
                      cross_send.at[k - 1, c], cross_recv.at[n_chips - k - 1, c], tp=across(k))

    def project(c):
        here = rows_of(c, CHUNK)
        pieces = [att[here, :]]
        for h in range(ret):
            both = jnp.concatenate([fterm[h, c], bterm[h, c]], axis=0).astype(BF16)
            combined = rloc[h, here, :] + mm(qfb[h, here, :], both)
            centered = combined - jnp.mean(combined, axis=1, keepdims=True)
            normed = centered * lax.rsqrt(jnp.mean(centered * centered, axis=1, keepdims=True) + NORM_EPS)
            gate = gs[here, h * RV:(h + 1) * RV].astype(F32)
            pieces.append((gate / (1.0 + jnp.exp(-gate)) * normed).astype(BF16))
        mixed = jnp.concatenate(pieces, axis=1)
        for k in list(range(1, n_chips)) + [0]:
            owner = lax.rem(chip + k, n_chips) * 2
            s_part[k, here, :] = mm(mixed, w_out[owner + 1 - core]).astype(BF16)
            acc[k, here, :] = mm(mixed, w_out[owner + core])
            part_copy(k, c).start()

    def relay(c):
        here = rows_of(c, CHUNK)
        for k in range(1, n_chips):
            part_copy(k, c).wait_recv()
            s_cross[k - 1, here, :] = (acc[k, here, :] + r_part[k, here, :].astype(F32)).astype(BF16)
            cross_copy(k, c).start()

    def mix_body(c, carry):
        @pl.when(c < chunks)
        def _():
            project(c)

        @pl.when(c > 0)
        def _():
            relay(c - 1)

        return carry

    lax.fori_loop(0, chunks + 1, mix_body, 0)

    def last_body(c, carry):
        here = rows_of(c, CHUNK)
        part_copy(0, c).wait_recv()
        total = acc[0, here, :] + r_part[0, here, :].astype(F32)
        for k in range(1, n_chips):
            cross_copy(k, c).wait_recv()
        for k in range(1, n_chips):
            total = total + r_cross[k - 1, here, :].astype(F32)
        out[here, :] = total.astype(BF16)
        return carry

    lax.fori_loop(0, chunks, last_body, 0)

    def sent(c, carry):
        own_part(c).wait_send()
        for k in range(1, n_chips):
            own_cross(c, k).wait_send()
            arrival(c, across(k), n_chips - 1 + k).wait_send()
            cross_copy(k, c).wait_send()
        for k in range(n_chips):
            part_copy(k, c).wait_send()
        return carry

    lax.fori_loop(0, chunks, sent, 0)
    for k in range(1, n_sp):
        log_copy(k).wait_send()

    def sent_total(d, carry):
        total_arrival(d).wait_send()
        return carry

    lax.fori_loop(sp + 1, n_sp, sent_total, 0)
    lax.fori_loop(0, sp, sent_total, 0)


def body(n_sp, n_tp, tokens, norm_gain, w_q, w_k, w_v, w_rq, w_rk, w_rv, w_rg, att_sink,
         decay_log, init_state, out_att, out_ret):
    rows, chan = tokens.shape
    width = n_tp * chan
    ret = decay_log.shape[0]
    heads = att_sink.shape[0]
    kv_cols = w_k.shape[1]
    kv = kv_cols // HD
    chunks = rows // CHUNK
    n_chips = n_tp // 2
    weights = (w_q, w_k, w_v, w_rq, w_rk, w_rv, w_rg)
    names = ("q", "k", "v", "rq", "rk", "rv", "g")
    cols = [w.shape[1] for w in weights]
    joined = all(count % 128 == 0 for count in cols)
    places, dots = [], []
    if joined:
        buffers = [sum(cols)]
        at = 0
        for count in cols:
            places.append((0, at, count))
            at += count
        for group in ((0,), (1, 2), (3, 4), (5,), (6,)):
            dots.append((0, places[group[0]][1], sum(cols[i] for i in group),
                         tuple((names[i], cols[i]) for i in group)))
    else:
        buffers = cols
        for i, count in enumerate(cols):
            places.append((i, 0, count))
            dots.append((i, 0, count, ((names[i], count),)))
    cfg = dict(n_sp=n_sp, n_tp=n_tp, n_chips=n_chips, chunks=chunks, chan=chan, heads=heads,
               ret=ret, kv=kv, buffers=buffers, places=places, dots=dots, joined=joined)
    outer = rope_tables(n_sp * chunks, CHUNK, ret)
    inner = rope_tables(CHUNK, 1, ret)
    vmem = pl.BlockSpec(memory_space=pltpu.VMEM)
    anyw = pl.BlockSpec(memory_space=pl.ANY)
    smem = pl.BlockSpec(memory_space=pltpu.SMEM)
    dma = pltpu.SemaphoreType.DMA
    mixed_rows = heads * HD + ret * RV
    others = max(n_chips - 1, 1)
    scratch = [pltpu.VMEM((width, count), BF16) for count in buffers] + [
        pltpu.VMEM((n_tp, mixed_rows, chan), BF16),
        pltpu.VMEM((n_tp, rows, chan), BF16),
        pltpu.VMEM((CHUNK, width), BF16),
        pltpu.VMEM((rows, heads * HD), BF16),
        pltpu.VMEM((rows + 2 * WINDOW, kv_cols), BF16),
        pltpu.VMEM((rows + 2 * WINDOW, kv_cols), BF16),
        pltpu.VMEM((rows, heads * HD), BF16),
        pltpu.VMEM((ret, rows, 2 * RK), BF16),
        pltpu.VMEM((ret, rows, RV), F32),
        pltpu.VMEM((rows, ret * RV), BF16),
        pltpu.VMEM((ret, chunks, RK, RV), F32),
        pltpu.VMEM((ret, chunks, RK, RV), F32),
        pltpu.VMEM((ret, chunks, 8, 128), F32),
        pltpu.VMEM((ret, RK, RV), BF16),
        pltpu.VMEM((ret, RK, RV), BF16),
        pltpu.VMEM((n_sp, ret, RK, RV), BF16),
        pltpu.VMEM((n_sp, ret, 8, 128), F32),
        pltpu.VMEM((2, ret, RK, RV), F32),
        pltpu.VMEM((n_chips, rows, chan), F32),
        pltpu.VMEM((n_chips, rows, chan), BF16),
        pltpu.VMEM((n_chips, rows, chan), BF16),
        pltpu.VMEM((others, rows, chan), BF16),
        pltpu.VMEM((others, rows, chan), BF16),
        dma((7,)), dma((n_tp, 2)), dma,
        dma((2 * n_chips, chunks)), dma((n_tp, chunks)),
        dma((2, 2)), dma((2, 2)),
        dma((n_sp,)), dma((n_sp,)),
        dma((n_sp,)), dma((n_sp,)),
        dma((n_chips, chunks)), dma((n_chips, chunks)),
        dma((others, chunks)), dma((others, chunks)),
    ]
    return pl.pallas_call(
        functools.partial(kernel, cfg),
        out_shape=jax.ShapeDtypeStruct((rows, chan), BF16),
        in_specs=[anyw, vmem] + [anyw] * 7 + [smem, vmem, vmem, anyw, anyw] + [vmem] * 4,
        out_specs=vmem,
        scratch_shapes=scratch,
        compiler_params=pltpu.CompilerParams(
            collective_id=0, has_side_effects=True, vmem_limit_bytes=60 * 1024 * 1024),
    )(tokens, norm_gain.reshape(1, width), *weights, att_sink, decay_log, init_state,
      out_att, out_ret, *(jnp.asarray(t) for t in outer), *(jnp.asarray(t) for t in inner))


def solution(mesh):
    n_sp, n_tp = mesh.shape["sp"], mesh.shape["tp"]
    in_specs = (
        P("sp", "tp"),
        P(),
        P(None, "tp"),
        P(None, "tp"),
        P(None, "tp"),
        P(None, "tp"),
        P(None, "tp"),
        P(None, "tp"),
        P(None, "tp"),
        P("tp"),
        P("tp", "sp"),
        P(None, "tp", None, None),
        P("tp", None),
        P("tp", None),
    )
    return jax.shard_map(functools.partial(body, n_sp, n_tp), mesh=mesh, in_specs=in_specs,
                         out_specs=P("sp", "tp"), check_vma=False)
```

time: 205 us -> 78 us (0.38)
  Pallas kernels: 0 us -> 75.6 us
  blocking collectives: 54.6 us -> 0 us
  waiting for transfers between devices: 45.1 us -> 0 us
  matrix products: 38.4 us -> 0 us
  local copies, waits for them, and re-layouts: 28 us -> 2.26 us
  other arithmetic: 20.3 us -> 0 us
  between operations: 14.8 us -> 0.01 us
  starting transfers between devices: 3.22 us -> 0 us
    pallas_call x0 -> x1, Pallas kernels: none -> 75.6 us  [body(): pl.pallas_call(functools.partial(kernel, cfg), out_shape=jax.ShapeDtypeSt...]
    reduce_scatter x1 -> x0, waiting for transfers between devices: 44.3 us -> none  [body(): lax.psum_scatter((att_part + lax.dot_general(out_ret, ret_out, contract_d...]
    dot_general x19 -> x0, matrix products: 38.4 us -> none  [the longest x1 8.95 us: body(): proj_sums = jnp.dot(scaled, joined, preferred_element_type=jnp.float32)]
    all_gather x1 -> x0, blocking collectives: 31.5 us -> none  [body(): lax.all_gather(jnp.stack([fwd_total, bwd_total]).astype(jnp.bfloat16), 'sp')]
    unnamed x1 -> x0, blocking collectives: 23.1 us -> none
    unnamed x84 -> x1, local copies, waits for them, and re-layouts: 11.8 us -> 2.26 us
    slice x11 -> x0, local copies, waits for them, and re-layouts: 7.81 us -> none  [the longest x3 2.76 us: body(): query_block = queries[first_row:first_row + block_rows]]
    reduce_sum x4 -> x0, other arithmetic: 5.92 us -> none  [the longest x1 3.07 us: body(): squares = jnp.sum(piece_f * piece_f, axis=1)]
  transfers between devices with their start and end apart: 4 -> 0, of which waited for: 1 -> 0; matrix products, arithmetic and copies ran while one was open for 22% -> 0% of each run, Pallas kernels for 0% -> 0%
where the time goes in v2:
time: 78 us; the launch traced here: 77.8 us
  Pallas kernels  75.6 us (97%)
  local copies, waits for them, and re-layouts  2.26 us (3%)
    pallas_call x1, Pallas kernels, body(): pl.pallas_call(functools.partial(kernel, cfg), out_shape=jax.ShapeDtypeSt...  75.6 us
    unnamed x1, local copies, waits for them, and re-layouts  2.26 us

profile of v2, /device:TPU:0, one launch (start us, length us, event | category | flops | bytes accessed | tf_op | source)
XLA Modules:
  0.0 77.8 jit_solution(3037172114066930370)
XLA Ops:
  0.0 75.6 %shard_map.172 = bf16[1024,512]{1,0:T(8,128)(2,1)} custom-call(bf16[1024,512]{1,0:T(8,128)(2,1)} %refs_0_.1, f32[1,2048]{1,0:T(1,128)} %bitcast.1, bf16[2048,256]{1,0:T(8,128)(2,1)} %refs_2_.1, bf16[2048,128]{1,0:T(8,128)(2,1)} %refs_3_.1, bf16[2048,128]{1,0:T(8,128)(2,1)} %refs_4_.1, bf16[2048,128]{1,0:T(8,128)(2,1)} %refs_5_.1, bf16[2048,128]{1,0:T(8,128)(2,1)} %refs_6_.1, ...), custom_call_target="tpu_custom_call" | custom-call | tf_op jit(solution)/shard_map/pallas_call | solution.py:476
  75.6 2.3 %copy.20 = bf16[1024,512]{1,0:T(8,128)(2,1)} copy(bf16[1024,512]{1,0:T(8,128)(2,1)} %shard_map.172) | data formatting | bytes 2097152

commit v3 on v2

--- a/solution.py
+++ b/solution.py
@@ -13,6 +13,7 @@
 RV = 128
 WINDOW = 128
 CHUNK = 256
+MIX = 128
 NORM_EPS = 1e-06
 ROPE_BASE = 10000.0
 F32 = jnp.float32
@@ -176,12 +177,21 @@
                 done.append(result[j * 128:(j + 1) * 128])
         att[here, :] = jnp.concatenate(done, axis=1).astype(BF16)
 
+    per = CHUNK // 128
+
     def chunk_body(c, carry):
         here = rows_of(c, CHUNK)
         for k in range(1, n_chips):
             slot = across(k)
             arrival(c, slot).wait_recv()
             arrival(c, slot, n_chips - 1 + k).start()
+        for j in range(per):
+            block = per * (c - 1) - 1 + j
+
+            @pl.when(block > 0)
+            def _():
+                attend(block)
+
         arrival(c, partner).wait_recv()
         for k in range(1, n_chips):
             arrival(c, lax.rem(chip + k, n_chips) * 2 + 1 - core).wait_recv()
@@ -231,11 +241,6 @@
             bterm[h, c] = terms[RK:]
             blog[h, c] = jnp.broadcast_to(total, (8, 128))
 
-        @pl.when(c > 0)
-        def _():
-            attend(2 * c - 1)
-            attend(2 * c)
-
         @pl.when(c == 0)
         def _():
             for k in range(1, n_sp):
@@ -276,10 +281,15 @@
     lax.fori_loop(sp + 1, n_sp, send_f, 0)
     lax.fori_loop(0, sp, send_b, 0)
 
+    def late(i, carry):
+        attend(i)
+        return carry
+
+    lax.fori_loop(max(per * (chunks - 1) - 1, 1), per * chunks - 1, late, 0)
     for copy in halos:
         copy.wait()
     attend(0)
-    attend(2 * chunks - 1)
+    attend(per * chunks - 1)
     for copy in o_copies:
         copy.wait()
 
@@ -321,20 +331,23 @@
             bterm[h, r] = back
             back = jnp.exp(blog[h, r, 0:1, :]) * back + term
 
+    mixes = rows // MIX
+
     def part_copy(k, c):
-        return remote(s_part.at[k, rows_of(c, CHUNK), :], r_part.at[k, rows_of(c, CHUNK), :],
+        return remote(s_part.at[k, rows_of(c, MIX), :], r_part.at[k, rows_of(c, MIX), :],
                       part_send.at[k, c], part_recv.at[k, c], tp=partner)
 
     def cross_copy(k, c):
-        return remote(s_cross.at[k - 1, rows_of(c, CHUNK), :],
-                      r_cross.at[n_chips - k - 1, rows_of(c, CHUNK), :],
+        return remote(s_cross.at[k - 1, rows_of(c, MIX), :],
+                      r_cross.at[n_chips - k - 1, rows_of(c, MIX), :],
                       cross_send.at[k - 1, c], cross_recv.at[n_chips - k - 1, c], tp=across(k))
 
     def project(c):
-        here = rows_of(c, CHUNK)
+        here = rows_of(c, MIX)
+        at = lax.div(c, CHUNK // MIX)
         pieces = [att[here, :]]
         for h in range(ret):
-            both = jnp.concatenate([fterm[h, c], bterm[h, c]], axis=0).astype(BF16)
+            both = jnp.concatenate([fterm[h, at], bterm[h, at]], axis=0).astype(BF16)
             combined = rloc[h, here, :] + mm(qfb[h, here, :], both)
             centered = combined - jnp.mean(combined, axis=1, keepdims=True)
             normed = centered * lax.rsqrt(jnp.mean(centered * centered, axis=1, keepdims=True) + NORM_EPS)
@@ -348,14 +361,14 @@
             part_copy(k, c).start()
 
     def relay(c):
-        here = rows_of(c, CHUNK)
+        here = rows_of(c, MIX)
         for k in range(1, n_chips):
             part_copy(k, c).wait_recv()
             s_cross[k - 1, here, :] = (acc[k, here, :] + r_part[k, here, :].astype(F32)).astype(BF16)
             cross_copy(k, c).start()
 
     def mix_body(c, carry):
-        @pl.when(c < chunks)
+        @pl.when(c < mixes)
         def _():
             project(c)
 
@@ -365,10 +378,10 @@
 
         return carry
 
-    lax.fori_loop(0, chunks + 1, mix_body, 0)
+    lax.fori_loop(0, mixes + 1, mix_body, 0)
 
     def last_body(c, carry):
-        here = rows_of(c, CHUNK)
+        here = rows_of(c, MIX)
         part_copy(0, c).wait_recv()
         total = acc[0, here, :] + r_part[0, here, :].astype(F32)
         for k in range(1, n_chips):
@@ -378,19 +391,24 @@
         out[here, :] = total.astype(BF16)
         return carry
 
-    lax.fori_loop(0, chunks, last_body, 0)
+    lax.fori_loop(0, mixes, last_body, 0)
 
     def sent(c, carry):
         own_part(c).wait_send()
         for k in range(1, n_chips):
             own_cross(c, k).wait_send()
             arrival(c, across(k), n_chips - 1 + k).wait_send()
+        return carry
+
+    def sent_mix(c, carry):
+        for k in range(1, n_chips):
             cross_copy(k, c).wait_send()
         for k in range(n_chips):
             part_copy(k, c).wait_send()
         return carry
 
     lax.fori_loop(0, chunks, sent, 0)
+    lax.fori_loop(0, mixes, sent_mix, 0)
     for k in range(1, n_sp):
         log_copy(k).wait_send()
 
@@ -470,8 +488,8 @@
         dma((2, 2)), dma((2, 2)),
         dma((n_sp,)), dma((n_sp,)),
         dma((n_sp,)), dma((n_sp,)),
-        dma((n_chips, chunks)), dma((n_chips, chunks)),
-        dma((others, chunks)), dma((others, chunks)),
+        dma((n_chips, rows // MIX)), dma((n_chips, rows // MIX)),
+        dma((others, rows // MIX)), dma((others, rows // MIX)),
     ]
     return pl.pallas_call(
         functools.partial(kernel, cfg),

time: 78 us -> 74.6 us (0.956)
  Pallas kernels: 75.6 us -> 72.1 us
    pallas_call x1, Pallas kernels: 75.6 us -> 72.1 us  [body(): pl.pallas_call(functools.partial(kernel, cfg), out_shape=jax.ShapeDtypeSt...]
where the time goes in v3:
time: 74.6 us; the launch traced here: 74.4 us
  Pallas kernels  72.1 us (97%)
  local copies, waits for them, and re-layouts  2.26 us (3%)
    pallas_call x1, Pallas kernels, body(): pl.pallas_call(functools.partial(kernel, cfg), out_shape=jax.ShapeDtypeSt...  72.1 us
    unnamed x1, local copies, waits for them, and re-layouts  2.26 us

profile of v3, /device:TPU:0, one launch (start us, length us, event | category | flops | bytes accessed | tf_op | source)
XLA Modules:
  0.0 74.4 jit_solution(14349814601842197970)
XLA Ops:
  0.0 72.1 %shard_map.172 = bf16[1024,512]{1,0:T(8,128)(2,1)} custom-call(bf16[1024,512]{1,0:T(8,128)(2,1)} %refs_0_.1, f32[1,2048]{1,0:T(1,128)} %bitcast.1, bf16[2048,256]{1,0:T(8,128)(2,1)} %refs_2_.1, bf16[2048,128]{1,0:T(8,128)(2,1)} %refs_3_.1, bf16[2048,128]{1,0:T(8,128)(2,1)} %refs_4_.1, bf16[2048,128]{1,0:T(8,128)(2,1)} %refs_5_.1, bf16[2048,128]{1,0:T(8,128)(2,1)} %refs_6_.1, ...), custom_call_target="tpu_custom_call" | custom-call | tf_op jit(solution)/shard_map/pallas_call | solution.py:494
  72.1 2.3 %copy.20 = bf16[1024,512]{1,0:T(8,128)(2,1)} copy(bf16[1024,512]{1,0:T(8,128)(2,1)} %shard_map.172) | data formatting | bytes 2097152
